TPU v7x, 512 devices: a whole 4x4x16 slice. The times are simulated.
512 devices in a mesh: tp: 64 (over z, y), dp: 8 (over x, core).
Axes of the slice: x: 4, y: 4, z: 16, core: 2. Of those that a mesh axis runs over, the one named last changes fastest.
Arguments:
- resid: bfloat16 [256, 2048], P('dp', 'tp'), may hold values from -6 to 6
- norm_gain: float32 [2, 2048], replicated, may hold values from 0.1 to 1.9
- w_query: bfloat16 [2, 2048, 2048], P(None, 'dp', 'tp'), may hold values from -0.125 to 0.125
- w_forget: bfloat16 [2, 2048, 2048], P(None, 'dp', 'tp'), may hold values from -0.125 to 0.125
- w_value: bfloat16 [2, 2048, 16, 128], P(None, 'dp', None, 'tp'), may hold values from -0.125 to 0.125
- w_gate: bfloat16 [2, 2048, 16, 128], P(None, 'dp', None, 'tp'), may hold values from -0.125 to 0.125
- gate_floor: float32 [2, 2048], replicated, may hold values from 0 to 0.9
- states: float32 [2, 256, 16, 128, 128], P(None, 'dp', None, 'tp'), may hold values from -1 to 1
- out_gain: float32 [2, 16, 128], P(None, None, 'tp'), may hold values from 0.1 to 1.9
- w_out: bfloat16 [2, 16, 128, 2048], P(None, None, 'tp'), may hold values from -0.125 to 0.125
Outputs:
- new_resid: bfloat16 [256, 2048], P('dp', 'tp')
- new_states: float32 [2, 256, 16, 128, 128], P(None, 'dp', None, 'tp')
All inputs are finite; a program needn't handle non-finite values.
Results may differ from a plain program's by a relative error of at most 0.029.
Values may be sent and summed in bfloat16 or wider, within the bound.
A program may use at most 64 MiB of HBM per device.

v0:
```python
import jax
import jax.numpy as jnp
from jax import lax
from jax.sharding import PartitionSpec as P

BLOCKS = 2


epsilon = 1e-06


def sent_to_all(value, axis):
    length = lax.axis_size(axis)
    return lax.all_to_all(
        jnp.broadcast_to(value[None], (length, *value.shape)), axis, 0, 0, tiled=True
    )


def in_order(parts, dim):
    shape = list(parts.shape[1:])
    shape[dim] *= parts.shape[0]
    return jnp.moveaxis(parts, 0, dim).reshape(shape)


def gather_directly(value, axis, dim):
    parts = sent_to_all(value, axis)
    return in_order(parts, dim)


def in_one_piece(arrays, axis, dim, along):
    ends, at = ([], 0)
    for a in arrays[:-1]:
        at += a.shape[along]
        ends.append(at)
    both = jnp.concatenate(arrays, axis=along)
    return tuple(jnp.split(lax.all_gather(both, axis, axis=dim, tiled=True), ends, axis=along))


def rows_first(arrays, axis, dims):
    turned = [jnp.moveaxis(a, dim, 0) for a, dim in zip(arrays, dims)]
    both = jnp.concatenate([t.reshape(len(t), -1) for t in turned], axis=1)
    out, at, finished = (lax.all_gather(both, axis, axis=0, tiled=True), 0, [])
    for t, dim in zip(turned, dims):
        share = out[:, at : at + t[0].size].reshape(-1, *t.shape[1:])
        finished.append(jnp.moveaxis(share, 0, dim))
        at += t[0].size
    return tuple(finished)


def of_everyone(value, axis):
    everything = sent_to_all(value, axis)
    return jnp.sum(everything, axis=0)


def in_blocks(value, dim, length):
    before, after = (value.shape[:dim], value.shape[dim + 1 :])
    return jnp.moveaxis(value.reshape(*before, length, -1, *after), dim, 0)


def summed_on_arrival(value, axis, dim):
    parts = in_blocks(value, dim, lax.axis_size(axis))
    arrived = lax.all_to_all(parts, axis, split_axis=0, concat_axis=0, tiled=True)
    return arrived.sum(axis=0)


def shards(
    resid, norm_gain, w_query, w_forget, w_value, w_gate, gate_floor, states, out_gain, w_out
):
    residual = resid
    seq_local = resid.shape[0]
    heads = states.shape[2]
    slice_cols = states.shape[3]
    head_dim = states.shape[4]
    row_count = w_query.shape[1]
    new_list = []
    for layer in range(BLOCKS):
        gathered = gather_directly(residual, "tp", 1)
        resid_f32 = gathered.astype(jnp.float32)
        inv_rms = lax.rsqrt(jnp.mean(resid_f32 * resid_f32, axis=1, keepdims=True) + epsilon)
        scaled = (resid_f32 * norm_gain[layer]).astype(jnp.bfloat16)
        query_rows = w_query[layer]
        forget_rows = w_forget[layer]
        value_rows = w_value[layer].reshape(row_count, -1)
        gate_rows = w_gate[layer].reshape(row_count, -1)
        zero_sums = (
            jnp.zeros((seq_local, query_rows.shape[1]), jnp.float32),
            jnp.zeros((seq_local, forget_rows.shape[1]), jnp.float32),
            jnp.zeros((seq_local, value_rows.shape[1]), jnp.float32),
            jnp.zeros((seq_local, gate_rows.shape[1]), jnp.float32),
        )
        totals = zero_sums
        pieces = in_one_piece((query_rows, forget_rows, value_rows, gate_rows), "dp", 0, 1)
        segments = pieces[0].shape[0] // row_count
        for part_index in range(segments):
            columns = lax.dynamic_slice_in_dim(scaled, part_index * row_count, row_count, 1)
            lo_row = part_index * row_count
            totals = tuple(
                (
                    total
                    + lax.optimization_barrier(
                        jnp.dot(
                            columns,
                            segment[lo_row : lo_row + row_count],
                            preferred_element_type=jnp.float32,
                        ).astype(jnp.bfloat16)
                    ).astype(jnp.float32)
                    for total, segment in zip(totals, pieces)
                )
            )
        queries, forget_pre, values, gate_pre = [
            (summed * inv_rms).astype(jnp.bfloat16) for summed in totals
        ]
        query_all, forget_all = rows_first((queries, forget_pre), "tp", (1, 1))
        floor_now = gate_floor[layer]
        keep = floor_now + (1.0 - floor_now) * jax.nn.sigmoid(forget_all.astype(jnp.float32))
        keep = keep.reshape(seq_local, heads, head_dim)
        value_f32 = values.astype(jnp.float32).reshape(seq_local, heads, slice_cols)
        state_new = (
            keep[:, :, None, :] * states[layer]
            + (1.0 - keep)[:, :, None, :] * value_f32[:, :, :, None]
        )
        query_f32 = query_all.astype(jnp.float32).reshape(seq_local, heads, head_dim)
        readout = jnp.sum(query_f32[:, :, None, :] * state_new, axis=3)
        power_sum = of_everyone(jnp.sum(readout * readout, axis=2), "tp")
        mean_square = power_sum[..., None] / head_dim
        gate_f32 = gate_pre.astype(jnp.float32).reshape(seq_local, heads, slice_cols)
        normed = (
            readout * lax.rsqrt(mean_square + epsilon) * out_gain[layer] * jax.nn.silu(gate_f32)
        ).astype(jnp.bfloat16)
        flattened = normed.reshape(seq_local, heads * slice_cols)
        weight_out = w_out[layer].reshape(heads * slice_cols, -1)
        branch = summed_on_arrival(
            lax.dot_general(
                weight_out, flattened, (((0,), (1,)), ((), ())), preferred_element_type=jnp.float32
            ),
            "tp",
            0,
        )
        residual = (residual.astype(jnp.float32) + branch.T).astype(jnp.bfloat16)
        new_list.append(state_new)
    return (residual, jnp.stack(new_list))


def solution(mesh):
    return jax.shard_map(
        shards,
        mesh=mesh,
        in_specs=(
            P("dp", "tp"),
            P(),
            P(None, "dp", "tp"),
            P(None, "dp", "tp"),
            P(None, "dp", None, "tp"),
            P(None, "dp", None, "tp"),
            P(),
            P(None, "dp", None, "tp", None),
            P(None, None, "tp"),
            P(None, None, "tp", None),
        ),
        out_specs=(P("dp", "tp"), P(None, "dp", None, "tp", None)),
        check_vma=False,
    )
```

profile of v0, /device:TPU:6, one launch (start us, length us, event | category | flops | bytes accessed | tf_op | source)
XLA Modules:
  0.0 415.3 jit_solution(12405203772914550517)
XLA Ops:
  0.6 0.8 broadcast_in_dim.8
  1.4 1.1 reshape.98
  2.5 18.9 %all-to-all-start = ((bf16[64,2,512]{2,1,0:T(2,128)(2,1)}), bf16[64,2,512]{2,1,0:T(2,128)(2,1)S(1)}, u32[]{:S(2)}, u32[]{:S(2)}) async-start(bf16[64,2,512]{2,1,0:T(2,128)(2,1)} %reshape.98), calls=%async_computation | async-start | bytes 262144 | tf_op jit(solution)/shard_map/all_to_all | solution.py:14
  21.4 0.6 fusion.167
  22.1 0.6 fusion.165
  22.8 0.7 copy-done.15
  23.5 0.6 fusion.166
  24.4 0.5 copy-done.18
  24.9 0.6 slice_bitcast_fusion.2
  25.6 13.1 %all_gather.12 = bf16[2048,128]{0,1:T(8,128)(2,1)S(1)} all-gather(bf16[256,128]{0,1:T(8,128)(2,1)S(1)} %pad_maximum_fusion.1), channel_id=1, replica_groups=mesh['tp'=64,'dp'=8] {'dp'}, dimensions={0}, use_global_device_ids=true | all-gather | bytes 589824 | tf_op jit(solution)/shard_map/all_gather | solution.py:36
  38.7 0.6 fusion.168
  39.3 0.7 mul.316
  40.0 0.7 copy-done.25
  40.7 0.6 broadcast_subtract_fusion.2
  42.0 0.6 copy.86
  42.6 0.5 reshape.92
  43.4 0.7 convolution_convert_fusion.39
  44.4 0.7 convolution_convert_fusion.38
  45.3 0.7 convolution_convert_fusion.37
  46.3 0.7 convolution_convert_fusion.36
  47.3 0.7 convolution_convert_fusion.35
  50.7 101.3 %all_gather.13 = bf16[2048,64]{1,0:T(8,128)(2,1)S(1)} all-gather(bf16[32,64]{1,0:T(8,128)(2,1)S(1)} %copy.87), channel_id=1, replica_groups=mesh['tp'=64,'dp'=8] {'tp'}, dimensions={0}, use_global_device_ids=true | all-gather | bytes 266240 | tf_op jit(solution)/shard_map/all_gather | solution.py:42
  153.0 0.7 copy-done.3
  153.8 1.4 fusion.7
  155.4 0.9 reshape.100
  156.3 12.3 %all-to-all-start.1 = ((f32[64,1,512]{2,1,0:T(1,128)}), f32[64,1,512]{2,1,0:T(1,128)S(1)}, u32[]{:S(2)}, u32[]{:S(2)}) async-start(f32[64,1,512]{2,1,0:T(1,128)} %reshape.100), calls=%async_computation.1 | async-start | bytes 262144 | tf_op jit(solution)/shard_map/all_to_all | solution.py:14
  169.0 18.0 %all-to-all-done.1 = f32[64,1,512]{2,1,0:T(1,128)S(1)} async-done(((f32[64,1,512]{2,1,0:T(1,128)}), f32[64,1,512]{2,1,0:T(1,128)S(1)}, u32[]{:S(2)}, u32[]{:S(2)}) %all-to-all-start.1) | async-done | bytes 131104 | tf_op jit(solution)/shard_map/all_to_all | solution.py:14
  187.0 0.5 broadcast.158
  187.5 0.9 reduce.4
  190.5 0.6 copy.125
  191.1 0.5 reshape.102
  191.6 22.7 %all_to_all.30 = f32[64,1,1024]{2,1,0:T(1,128)S(1)} all-to-all(f32[64,1,1024]{2,1,0:T(1,128)S(1)} %reshape.102), channel_id=1, replica_groups=mesh['tp'=64,'dp'=8] {'tp'}, dimensions={0} | all-to-all | bytes 524288 | tf_op jit(solution)/shard_map/all_to_all | solution.py:62
  214.3 1.2 reduce.5
  216.0 0.6 copy-done.13
  216.7 1.1 reshape.104
  217.7 4.7 %all-to-all-start.3 = ((bf16[64,2,512]{2,1,0:T(2,128)(2,1)}), bf16[64,2,512]{2,1,0:T(2,128)(2,1)S(1)}, u32[]{:S(2)}, u32[]{:S(2)}) async-start(bf16[64,2,512]{2,1,0:T(2,128)(2,1)} %reshape.104), calls=%async_computation.3 | async-start | bytes 262144 | tf_op jit(solution)/shard_map/all_to_all | solution.py:14
  222.6 0.7 mul.349
  223.2 0.7 copy-done.10
  224.0 0.7 reshape_squeeze.23
  224.7 13.1 %all_gather.14 = bf16[2048,128]{0,1:T(8,128)(2,1)S(1)} all-gather(bf16[256,128]{0,1:T(8,128)(2,1)S(1)} %pad_maximum_fusion.2), channel_id=1, replica_groups=mesh['tp'=64,'dp'=8] {'dp'}, dimensions={0}, use_global_device_ids=true | all-gather | bytes 589824 | tf_op jit(solution)/shard_map/all_gather | solution.py:36
  237.8 0.8 all-to-all-done.3
  239.3 0.6 copy.100
  239.9 0.5 reshape.95
  244.9 100.7 %all_gather.15 = bf16[2048,64]{1,0:T(8,128)(2,1)S(1)} all-gather(bf16[32,64]{1,0:T(8,128)(2,1)S(1)} %copy.101), channel_id=1, replica_groups=mesh['tp'=64,'dp'=8] {'tp'}, dimensions={0}, use_global_device_ids=true | all-gather | bytes 266240 | tf_op jit(solution)/shard_map/all_gather | solution.py:42
  345.8 1.0 copy.102
  347.0 0.5 copy-done.16
  347.7 0.9 copy-done.6
  348.6 1.3 fusion.4
  350.2 0.9 reshape.106
  351.1 12.4 %all-to-all-start.4 = ((f32[64,1,512]{2,1,0:T(1,128)}), f32[64,1,512]{2,1,0:T(1,128)S(1)}, u32[]{:S(2)}, u32[]{:S(2)}) async-start(f32[64,1,512]{2,1,0:T(1,128)} %reshape.106), calls=%async_computation.4 | async-start | bytes 262144 | tf_op jit(solution)/shard_map/all_to_all | solution.py:14
  363.5 0.8 convolution_convert_fusion.2
  364.3 0.8 convolution_convert_fusion.1
  365.2 0.8 convolution_convert_fusion
  366.0 15.6 %all-to-all-done.4 = f32[64,1,512]{2,1,0:T(1,128)S(1)} async-done(((f32[64,1,512]{2,1,0:T(1,128)}), f32[64,1,512]{2,1,0:T(1,128)S(1)}, u32[]{:S(2)}, u32[]{:S(2)}) %all-to-all-start.4) | async-done | bytes 131104 | tf_op jit(solution)/shard_map/all_to_all | solution.py:14
  381.6 0.9 reduce.6
  383.3 0.6 copy-done.7
  384.5 1.6 copy.124
  386.1 2.4 reshape.108
  388.5 5.9 %all-to-all-start.5 = ((f32[64,1,1024]{2,1,0:T(1,128)}), f32[64,1,1024]{2,1,0:T(1,128)S(1)}, u32[]{:S(2)}, u32[]{:S(2)}) async-start(f32[64,1,1024]{2,1,0:T(1,128)} %reshape.108), calls=%async_computation.5 | async-start | bytes 524288 | tf_op jit(solution)/shard_map/all_to_all | solution.py:62
  394.4 1.4 multiply_add_fusion.1
  395.8 1.5 pad_maximum_fusion
  397.3 15.7 %all-to-all-done.5 = f32[64,1,1024]{2,1,0:T(1,128)S(1)} async-done(((f32[64,1,1024]{2,1,0:T(1,128)}), f32[64,1,1024]{2,1,0:T(1,128)S(1)}, u32[]{:S(2)}, u32[]{:S(2)}) %all-to-all-start.5) | async-done | bytes 262176 | tf_op jit(solution)/shard_map/all_to_all | solution.py:62
  413.0 1.2 reduce.7
  414.7 0.6 fusion.80
  (187 shorter events, 17.1 us)
Async XLA Ops:
  1.4 20.0 %copy-start.26 = (f32[2,2048]{1,0:T(2,128)S(1)}, f32[2,2048]{1,0:T(2,128)}, u32[]{:S(2)}) copy-start(f32[2,2048]{1,0:T(2,128)} %param.11) | copy-start | bytes 49156
  2.5 21.7 %copy-start.8 = (bf16[2,16,2,2048]{3,2,1,0:T(2,128)(2,1)S(1)}, bf16[2,16,2,2048]{3,2,1,0:T(2,128)(2,1)}, u32[]{:S(2)}) copy-start(bf16[2,16,2,2048]{3,2,1,0:T(2,128)(2,1)} %param.19) | copy-start | bytes 786436
  2.5 38.8 %all-to-all-start = ((bf16[64,2,512]{2,1,0:T(2,128)(2,1)}), bf16[64,2,512]{2,1,0:T(2,128)(2,1)S(1)}, u32[]{:S(2)}, u32[]{:S(2)}) async-start(bf16[64,2,512]{2,1,0:T(2,128)(2,1)} %reshape.98), calls=%async_computation | async-start | bytes 262144 | tf_op jit(solution)/shard_map/all_to_all | solution.py:14
  21.4 0.8 copy-start.14
  22.8 0.8 copy-start.15
  24.2 0.8 copy-start.18
  24.2 0.8 copy-start.19
  25.6 13.1 %copy-start.30 = (f32[2,16,2]{1,2,0:T(2,128)S(1)}, f32[2,16,2]{1,2,0:T(2,128)}, u32[]{:S(2)}) copy-start(f32[2,16,2]{1,2,0:T(2,128)} %param.18) | copy-start | bytes 772
  40.0 0.7 copy-start.25
  49.8 0.6 copy-start.27
  50.7 102.2 %copy-start.1 = (f32[32,16,2]{2,1,0:T(8,128)}, f32[32,16,2]{2,1,0:T(8,128)S(1)}, u32[]{:S(2)}) copy-start(f32[32,16,2]{2,1,0:T(8,128)S(1)} %copy.91) | copy-start | bytes 12292
  152.6 1.2 copy-start
  152.9 0.7 copy-start.3
  156.3 30.7 %all-to-all-start.1 = ((f32[64,1,512]{2,1,0:T(1,128)}), f32[64,1,512]{2,1,0:T(1,128)S(1)}, u32[]{:S(2)}, u32[]{:S(2)}) async-start(f32[64,1,512]{2,1,0:T(1,128)} %reshape.100), calls=%async_computation.1 | async-start | bytes 262144 | tf_op jit(solution)/shard_map/all_to_all | solution.py:14
  189.0 0.7 copy-start.24
  189.0 0.7 copy-start.28
  189.0 0.7 copy-start.32
  189.2 0.7 copy-start.20
  189.2 0.7 copy-start.21
  189.2 0.7 copy-start.22
  189.2 0.7 copy-start.23
  215.9 0.7 copy-start.13
  216.7 5.8 %copy-start.29 = (f32[1,16,2]{1,2,0:T(2,128)S(1)}, f32[1,16,2]{1,2,0:T(2,128)}, u32[]{:S(2)}) copy-start(f32[1,16,2]{1,2,0:T(2,128)} %get-tuple-element.24) | copy-start | bytes 388
  217.7 20.9 %all-to-all-start.3 = ((bf16[64,2,512]{2,1,0:T(2,128)(2,1)}), bf16[64,2,512]{2,1,0:T(2,128)(2,1)S(1)}, u32[]{:S(2)}, u32[]{:S(2)}) async-start(bf16[64,2,512]{2,1,0:T(2,128)(2,1)} %reshape.104), calls=%async_computation.3 | async-start | bytes 262144 | tf_op jit(solution)/shard_map/all_to_all | solution.py:14
  222.5 0.8 copy-start.9
  223.2 0.7 copy-start.10
  224.0 0.7 copy-start.11
  224.0 0.7 copy-start.12
  237.8 6.4 %copy-start.5 = (bf16[2048,128]{0,1:T(8,128)(2,1)}, bf16[2048,128]{0,1:T(8,128)(2,1)S(1)}, u32[]{:S(2)}) copy-start(bf16[2048,128]{0,1:T(8,128)(2,1)S(1)} %all_gather.14) | copy-start | bytes 1572868
  239.9 0.7 copy-start.17
  346.8 0.7 copy-start.16
  347.7 1.0 copy-start.6
  351.1 30.5 %all-to-all-start.4 = ((f32[64,1,512]{2,1,0:T(1,128)}), f32[64,1,512]{2,1,0:T(1,128)S(1)}, u32[]{:S(2)}, u32[]{:S(2)}) async-start(f32[64,1,512]{2,1,0:T(1,128)} %reshape.106), calls=%async_computation.4 | async-start | bytes 262144 | tf_op jit(solution)/shard_map/all_to_all | solution.py:14
  383.0 0.9 copy-start.7
  383.2 0.7 copy-start.31
  388.5 5.9 %copy-start.2 = (f32[32,16,2]{2,1,0:T(8,128)S(1)}, f32[32,16,2]{2,1,0:T(8,128)}, u32[]{:S(2)}) copy-start(f32[32,16,2]{2,1,0:T(8,128)} %copy-done.1) | copy-start | bytes 12292
  388.5 5.9 %copy-start.4 = (f32[32,16,128]{2,1,0:T(8,128)S(1)}, f32[32,16,128]{2,1,0:T(8,128)}, u32[]{:S(2)}) copy-start(f32[32,16,128]{2,1,0:T(8,128)} %copy-done.3) | copy-start | bytes 786436
  388.5 24.5 %all-to-all-start.5 = ((f32[64,1,1024]{2,1,0:T(1,128)}), f32[64,1,1024]{2,1,0:T(1,128)S(1)}, u32[]{:S(2)}, u32[]{:S(2)}) async-start(f32[64,1,1024]{2,1,0:T(1,128)} %reshape.108), calls=%async_computation.5 | async-start | bytes 524288 | tf_op jit(solution)/shard_map/all_to_all | solution.py:62
where the time goes:
time: 417 us; the launch traced here: 415 us
  blocking collectives  251 us (60%)
  starting transfers between devices  54.2 us (13%)
  waiting for transfers between devices  50 us (12%)
  local copies, waits for them, and re-layouts  31.6 us (8%)
  other arithmetic  13.7 us (3%)
  matrix products  13.7 us (3%)
    all_gather x2, blocking collectives, rows_first(): out, at, finished = (lax.all_gather(both, axis, axis=0, tiled=True), 0, [])  202 us
    all_to_all x4, starting transfers between devices, sent_to_all(): lax.all_to_all(jnp.broadcast_to(value[None], (length, *value.shape)), axi...  48.3 us
    all_to_all x4, waiting for transfers between devices, sent_to_all(): lax.all_to_all(jnp.broadcast_to(value[None], (length, *value.shape)), axi...  34.3 us
    all_gather x2, blocking collectives, in_one_piece(): lax.all_gather(both, axis, axis=dim, tiled=True)  26.2 us
    all_to_all x1, blocking collectives, summed_on_arrival(): lax.all_to_all(parts, axis, split_axis=0, concat_axis=0, tiled=True)  22.7 us
    unnamed x84, local copies, waits for them, and re-layouts  16.5 us
    all_to_all x1, waiting for transfers between devices, summed_on_arrival(): lax.all_to_all(parts, axis, split_axis=0, concat_axis=0, tiled=True)  15.7 us
    dot_general x64, matrix products, shards(): jnp.dot(columns, segment[lo_row:lo_row + row_count], preferred_element_ty...  13.2 us
  transfers between devices with their start and end apart: 5, of which 4 were waited for; matrix products, arithmetic and copies ran while one was open for 3% of the time, Pallas kernels for 0%

commit v1 on v0

v1 whole, which is shorter than its diff:
```python
import functools

import jax
import jax.numpy as jnp
from jax import lax
from jax.experimental import pallas as pl
from jax.experimental.pallas import tpu as pltpu
from jax.sharding import PartitionSpec as P

MESH = pl.DeviceIdType.MESH
EPS = 1e-06
F32, BF16 = jnp.float32, jnp.bfloat16
NZ, NY, NDP = 16, 4, 8
PITCH = 24


def lanes():
    return lax.broadcasted_iota(jnp.int32, (8, 128), 1)


def turn(parts):
    group = lax.broadcasted_iota(jnp.int32, parts[0].shape, parts[0].ndim - 1) // 32
    axis = parts[0].ndim - 1
    out = []
    for g in range(4):
        acc = parts[g]
        for p in range(4):
            if p != g:
                acc = jnp.where(group == p, pltpu.roll(parts[p], (32 * (p - g)) % 128, axis), acc)
        out.append(acc)
    return out


def kernel(
    x_ref, gain_ref, wt_ref, floor_ref, og_ref, wo_ref, st_hbm,
    xo_ref, so_hbm,
    gx, gq, gg, gr, wt, wo, st, kq, xs, xres, x1b,
    sx, rx, sw, rw, so_s, so_r, lsem,
):
    tp = lax.axis_index("tp")
    dp = lax.axis_index("dp")
    z, y = tp // NY, tp % NY
    core = dp % 2
    zdist = (8, 7, 9, 6, 10, 5, 11, 4, 12, 3, 13, 2, 14, 1, 15)
    zi = [lax.rem(z + k, NZ) for k in zdist]
    zp = [{"tp": i * NY + y} for i in zi]
    yp = [{"tp": z * NY + lax.rem(y + k, NY)} for k in (2, 1, 3)]
    dpp = [{"dp": lax.rem(dp + k, NDP)} for k in (4, 3, 5, 2, 6, 1, 7)]
    mate = {"dp": dp + 1 - 2 * core}

    loads = [pltpu.make_async_copy(st_hbm.at[b], st.at[b], lsem.at[b]) for b in range(2)]
    for c in loads:
        c.start()

    bar = pltpu.get_barrier_semaphore()
    for p in zp + yp + dpp:
        pl.semaphore_signal(bar, inc=1, device_id=p, device_id_type=MESH)
    gx[0, y, z, 0] = x_ref[...]
    pl.semaphore_wait(bar, len(zp) + len(yp) + len(dpp))

    def send(src, dst, s, r, p):
        pltpu.make_async_remote_copy(src, dst, s, r, device_id=p, device_id_type=MESH).start()

    def arrived(ref, s, r):
        pltpu.make_async_remote_copy(ref, ref, s, r, device_id=mate, device_id_type=MESH).wait_recv()

    def left(ref, s, r):
        pltpu.make_async_remote_copy(ref, ref, s, r, device_id=mate, device_id_type=MESH).wait_send()

    def z_send(buf, i):
        for p in zp:
            send(buf.at[y, z], buf.at[y, z], sx.at[i, 0], rx.at[i, 0], p)

    def z_wait(buf, i):
        arrived(buf.at[0, pl.ds(0, NZ - 1)], sx.at[i, 0], rx.at[i, 0])

    def y_send(buf, i):
        for p in yp:
            send(buf.at[y], buf.at[y], sx.at[i, 1], rx.at[i, 1], p)

    def y_wait(buf, i):
        arrived(buf.at[pl.ds(0, NY - 1)], sx.at[i, 1], rx.at[i, 1])

    def all_left(buf, i):
        left(buf.at[0, pl.ds(0, NZ - 1)], sx.at[i, 0], rx.at[i, 0])
        left(buf.at[pl.ds(0, NY - 1)], sx.at[i, 1], rx.at[i, 1])

    z_send(gx.at[0], 0)
    for b in range(2):
        for p in dpp:
            send(wt_ref.at[b], wt.at[b, dp], sw.at[b], rw.at[b], p)
    for i, p in zip(zi, zp):
        send(wo_ref.at[core, i], wo.at[core, z, y], so_s.at[0], so_r.at[0], p)
    for b in range(2):
        wt[b, dp] = wt_ref[b]
    wo[core, z, y] = wo_ref[core, z]
    z_wait(gx.at[0], 0)
    y_send(gx.at[0], 0)
    arrived(wt.at[0, pl.ds(0, NDP - 1)], sw.at[0], rw.at[0])
    y_wait(gx.at[0], 0)

    for b in range(2):
        base = 4 * b
        if b == 0:
            tiles = turn([gx[0, i, :, 0].astype(F32) for i in range(NY)])
            for a in range(4):
                for k in range(NZ):
                    xres[k, 8 * a : 8 * a + 8, :] = tiles[a][k]
        else:
            tiles = [gx[1, a, :, 0].astype(F32) for a in range(NY)]
        inv = []
        for a in range(4):
            sq = jnp.sum(jnp.sum(tiles[a] * tiles[a], axis=0), axis=1, keepdims=True)
            inv.append(lax.rsqrt(sq / (NZ * 128) + EPS))
            for k in range(NZ):
                scaled = tiles[a][k] * gain_ref[b : b + 1, 128 * k : 128 * k + 128]
                xs[8 * a : 8 * a + 8, 128 * k : 128 * k + 128] = scaled.astype(BF16)
        inv = jnp.concatenate(inv, axis=0)
        if b == 1:
            arrived(wt.at[1, pl.ds(0, NDP - 1)], sw.at[1], rw.at[1])
        total = jnp.zeros((32, 128), F32)
        for d in range(NDP):
            part = lax.dot_general(
                xs[:, 256 * d : 256 * d + 256], wt[b, d], (((1,), (1,)), ((), ())), preferred_element_type=F32
            )
            total = total + part.astype(BF16).astype(F32)
        proj = (total * inv).astype(BF16).astype(F32)
        packed = turn([proj[8 * a : 8 * a + 8] for a in range(4)])
        gq[b, y, z, 0] = packed[0].astype(BF16)
        gq[b, y, z, 1] = packed[1].astype(BF16)
        z_send(gq.at[b], base + 1)
        gate = packed[3]
        gg[b, y, z, 0] = (og_ref[b : b + 1, :] * (gate / (1.0 + jnp.exp(-gate)))).astype(BF16)
        z_send(gg.at[b], base + 2)
        if b == 0:
            arrived(wo.at[0, pl.ds(0, NZ - 1), 0], so_s.at[0], so_r.at[0])
            for p in yp:
                send(wo.at[core, :, y], wo.at[core, :, y], so_s.at[1], so_r.at[1], p)
        vt = jnp.transpose(jnp.concatenate([proj, jnp.zeros((96, 128), F32)], axis=0))
        z_wait(gq.at[b], base + 1)
        y_send(gq.at[b], base + 1)
        z_wait(gg.at[b], base + 2)
        y_send(gg.at[b], base + 2)
        y_wait(gq.at[b], base + 1)
        forget = turn([gq[b, i, :, 1].astype(F32) for i in range(NY)])
        query = turn([gq[b, i, :, 0].astype(F32) for i in range(NY)])
        for a in range(4):
            for k in range(NZ):
                low = floor_ref[b : b + 1, 128 * k : 128 * k + 128]
                keep = low + (1.0 - low) * (1.0 / (1.0 + jnp.exp(-forget[a][k])))
                kq[0, pl.ds(8 * a * PITCH + k, 8, stride=PITCH), :] = keep
                kq[1, pl.ds(8 * a * PITCH + k, 8, stride=PITCH), :] = query[a][k]
        loads[b].wait()
        lane = lanes()
        read = [[jnp.zeros((8, 128), F32) for _ in range(2)] for _ in range(2)]
        for s in range(32):
            for hh in range(2):
                keep = kq[0, s * PITCH + 8 * hh : s * PITCH + 8 * hh + 8, :]
                quer = kq[1, s * PITCH + 8 * hh : s * PITCH + 8 * hh + 8, :]
                rest = 1.0 - keep
                for j in range(2):
                    rows = pl.ds(s * 32 + hh * 16 + j, 8, stride=2)
                    row0 = 64 + j * 16 + hh * 8
                    new = keep * st[b, rows, :] + rest * vt[row0 : row0 + 8, s : s + 1]
                    st[b, rows, :] = new
                    red = jnp.sum(quer * new, axis=1, keepdims=True)
                    read[j][hh] = jnp.where(lane == s, red, read[j][hh])
        rt = jnp.concatenate([read[0][0], read[0][1], read[1][0], read[1][1], jnp.zeros((96, 128), F32)], axis=0)
        rt = jnp.transpose(rt)
        tile = rt[0:8]
        for a in range(1, 4):
            tile = tile + pltpu.roll(rt[8 * a : 8 * a + 8], 32 * a, 1)
        gr[b, y, z, 0] = tile.astype(BF16)
        z_send(gr.at[b], base + 3)
        store = pltpu.make_async_copy(st.at[b], so_hbm.at[b], lsem.at[2 + b])
        store.start()
        if b == 0:
            first_store = store
            arrived(wo.at[0, pl.ds(0, NZ), pl.ds(0, NY - 1)], so_s.at[1], so_r.at[1])
            send(wo.at[core], wo.at[core], so_s.at[2], so_r.at[2], mate)
        y_wait(gg.at[b], base + 2)
        gate = turn([gg[b, i, :, 0].astype(F32) for i in range(NY)])
        z_wait(gr.at[b], base + 3)
        y_send(gr.at[b], base + 3)
        y_wait(gr.at[b], base + 3)
        read = turn([gr[b, i, :, 0].astype(F32) for i in range(NY)])
        for a in range(4):
            sq = jnp.sum(read[a] * read[a], axis=0)
            for shift in (64, 32, 16):
                sq = sq + pltpu.roll(sq, shift, 1)
            scale = lax.rsqrt(sq / 128.0 + EPS)
            for k in range(NZ):
                xs[8 * a : 8 * a + 8, 128 * k : 128 * k + 128] = (read[a][k] * scale * gate[a][k]).astype(BF16)
        if b == 0:
            arrived(wo.at[0], so_s.at[2], so_r.at[2])
        branch = jnp.dot(xs[...], wo[b].reshape(2048, 128), preferred_element_type=F32)
        if b == 0:
            fresh = (xres[z] + branch).astype(BF16).astype(F32)
            xres[0] = fresh
            for a in range(4):
                x1b[a] = fresh[8 * a : 8 * a + 8].astype(BF16)
            gx[1, y, z, 0] = x1b[y]
            z_send(gx.at[1], 4)
            z_wait(gx.at[1], 4)
            y_send(gx.at[1], 4)
            y_wait(gx.at[1], 4)
        else:
            fresh = xres[0] + branch
            mine = fresh
            for k in range(1, NY):
                mine = jnp.where(y == k, pltpu.roll(fresh, 128 - 32 * k, 1), mine)
            xo_ref[...] = mine[:, :32].astype(BF16)

    for b in range(2):
        all_left(gx.at[b], 4 * b)
        all_left(gq.at[b], 4 * b + 1)
        all_left(gg.at[b], 4 * b + 2)
        all_left(gr.at[b], 4 * b + 3)
        left(wt.at[b, pl.ds(0, NDP - 1)], sw.at[b], rw.at[b])
    left(wo.at[0, pl.ds(0, NZ - 1), 0], so_s.at[0], so_r.at[0])
    left(wo.at[0, pl.ds(0, NZ), pl.ds(0, NY - 1)], so_s.at[1], so_r.at[1])
    left(wo.at[0], so_s.at[2], so_r.at[2])
    first_store.wait()
    store.wait()


def shards(
    resid, norm_gain, w_query, w_forget, w_value, w_gate, gate_floor, states, out_gain, w_out
):
    seqs = resid.shape[0]
    x = resid.reshape(4, 8, 32).transpose(1, 0, 2).reshape(8, 128)
    value_t = w_value.transpose(0, 3, 2, 1).reshape(2, 32, 256)
    gate_t = w_gate.transpose(0, 3, 2, 1).reshape(2, 32, 256)
    wt = jnp.concatenate([w_query.transpose(0, 2, 1), w_forget.transpose(0, 2, 1), value_t, gate_t], axis=1)
    og = jnp.tile(out_gain.transpose(0, 2, 1).reshape(2, 32), (1, 4))
    wo = w_out.transpose(0, 2, 1, 3).reshape(2, 32, 16, 128).transpose(0, 2, 1, 3)
    st = states.reshape(2, seqs * 32, 128)
    vmem = pl.BlockSpec(memory_space=pltpu.VMEM)
    hbm = pl.BlockSpec(memory_space=pl.ANY)
    dma = pltpu.SemaphoreType.DMA
    new_resid, new_states = pl.pallas_call(
        kernel,
        out_shape=(jax.ShapeDtypeStruct((32, 32), BF16), jax.ShapeDtypeStruct(st.shape, F32)),
        in_specs=[vmem] * 6 + [hbm],
        out_specs=(vmem, hbm),
        scratch_shapes=[
            pltpu.VMEM((2, NY, NZ, 1, 8, 128), BF16),
            pltpu.VMEM((2, NY, NZ, 2, 8, 128), BF16),
            pltpu.VMEM((2, NY, NZ, 1, 8, 128), BF16),
            pltpu.VMEM((2, NY, NZ, 1, 8, 128), BF16),
            pltpu.VMEM((2, NDP, 128, 256), BF16),
            pltpu.VMEM((2, NZ, NY, 32, 128), BF16),
            pltpu.VMEM((2, 1024, 128), F32),
            pltpu.VMEM((2, 32 * PITCH, 128), F32),
            pltpu.VMEM((32, 2048), BF16),
            pltpu.VMEM((NZ, 32, 128), F32),
            pltpu.VMEM((4, 8, 128), BF16),
            dma((8, 2)),
            dma((8, 2)),
            dma((2,)),
            dma((2,)),
            dma((3,)),
            dma((3,)),
            dma((4,)),
        ],
        compiler_params=pltpu.CompilerParams(collective_id=0, has_side_effects=True),
        name="blocks",
    )(x, norm_gain, wt, gate_floor, og, wo, st)
    return new_resid, new_states.reshape(states.shape)


def solution(mesh):
    return jax.shard_map(
        shards,
        mesh=mesh,
        in_specs=(
            P("dp", "tp"),
            P(),
            P(None, "dp", "tp"),
            P(None, "dp", "tp"),
            P(None, "dp", None, "tp"),
            P(None, "dp", None, "tp"),
            P(),
            P(None, "dp", None, "tp", None),
            P(None, None, "tp"),
            P(None, None, "tp", None),
        ),
        out_specs=(P("dp", "tp"), P(None, "dp", None, "tp", None)),
        check_vma=False,
    )
```

time: 417 us -> 103 us (0.25)
  blocking collectives: 251 us -> 0 us
  Pallas kernels: 0 us -> 91.6 us
  starting transfers between devices: 54.2 us -> 0 us
  waiting for transfers between devices: 50 us -> 0 us
  local copies, waits for them, and re-layouts: 31.6 us -> 8.81 us
  matrix products: 13.7 us -> 0 us
  other arithmetic: 13.7 us -> 1.43 us
    all_gather x4 -> x0, blocking collectives: 228 us -> none  [the longest x2 202 us: rows_first(): out, at, finished = (lax.all_gather(both, axis, axis=0, tiled=True), 0, [])]
    pallas_call x0 -> x1, Pallas kernels: none -> 91.6 us  [shards(): pl.pallas_call(kernel, out_shape=(jax.ShapeDtypeStruct((32, 32), BF16), j...]
    all_to_all x5 -> x0, starting transfers between devices: 54.2 us -> none  [the longest x4 48.3 us: sent_to_all(): lax.all_to_all(jnp.broadcast_to(value[None], (length, *value.shape)), axi...]
    all_to_all x5 -> x0, waiting for transfers between devices: 50 us -> none  [the longest x4 34.3 us: sent_to_all(): lax.all_to_all(jnp.broadcast_to(value[None], (length, *value.shape)), axi...]
    all_to_all x1 -> x0, blocking collectives: 22.7 us -> none  [summed_on_arrival(): lax.all_to_all(parts, axis, split_axis=0, concat_axis=0, tiled=True)]
    dot_general x66 -> x0, matrix products: 13.7 us -> none  [the longest x64 13.2 us: shards(): jnp.dot(columns, segment[lo_row:lo_row + row_count], preferred_element_ty...]
    unnamed x84 -> x5, local copies, waits for them, and re-layouts: 16.5 us -> 3.6 us
    all_to_all x4 -> x0, other arithmetic: 4.37 us -> none  [the longest x2 2.49 us: summed_on_arrival(): lax.all_to_all(parts, axis, split_axis=0, concat_axis=0, tiled=True)]
  transfers between devices with their start and end apart: 5 -> 0, of which waited for: 4 -> 0; matrix products, arithmetic and copies ran while one was open for 3% -> 0% of each run, Pallas kernels for 0% -> 0%
where the time goes in v1:
time: 103 us
  Pallas kernels  91.6 us (89%)
  local copies, waits for them, and re-layouts  8.81 us (9%)
  other arithmetic  1.43 us (1%)
    pallas_call x1, Pallas kernels, shards(): pl.pallas_call(kernel, out_shape=(jax.ShapeDtypeStruct((32, 32), BF16), j...  91.6 us
    unnamed x5, local copies, waits for them, and re-layouts  3.6 us

profile of v1, /device:TPU:6, one launch (start us, length us, event | category | flops | bytes accessed | tf_op | source)
XLA Modules:
  0.0 102.5 jit_solution(17065534072599007727)
XLA Ops:
  0.6 0.0 copy-start
  0.6 0.8 tile.10
  1.4 0.7 tile.12.og_ref
  2.1 0.7 copy.24
  2.8 0.7 reshape.30.x_ref
  3.5 0.8 copy.16
  4.2 0.8 copy.17
  5.0 1.4 %pad_maximum_fusion.wt_ref = bf16[2,128,256]{2,1,0:T(8,128)(2,1)} fusion(bf16[2,32,256]{2,1,0:T(8,128)(2,1)S(1)} %bitcast.29, bf16[2,32,256]{2,1,0:T(8,128)(2,1)S(1)} %bitcast.28, bf16[2,32,256]{2,1,0:T(8,128)(2,1)} %bitcast.33, bf16[2,32,256]{2,1,0:T(8,128)(2,1)} %bitcast.34), kind=kLoop, calls=%fused_computation.1 | loop fusion | flops 524288 | bytes 262144 | tf_op jit(solution)/shard_map/concatenate | solution.py:234
  6.4 0.0 copy-done
  6.4 0.1 copy.18
  6.6 0.8 copy.23
  7.3 91.6 %blocks.1 = (bf16[32,32]{1,0:T(8,128)(2,1)}, f32[2,1024,128]{2,1,0:T(8,128)}) custom-call(bf16[8,128]{1,0:T(8,128)(2,1)} %reshape.30.x_ref, f32[2,2048]{1,0:T(2,128)} %gain_ref.1, bf16[2,128,256]{2,1,0:T(8,128)(2,1)} %pad_maximum_fusion.wt_ref, f32[2,2048]{1,0:T(2,128)} %floor_ref.1, f32[2,128]{1,0:T(2,128)} %tile.12.og_ref, ...), custom_call_target="tpu_custom_call" | custom-call | tf_op jit(solution)/shard_map/blocks/pallas_call | solution.py:241
  99.0 1.3 %copy.27 = bf16[32,32]{1,0:T(8,128)(2,1)} copy(bf16[32,32]{1,0:T(8,128)(2,1)} %get-tuple-element.8) | data formatting | bytes 4096
  100.3 2.3 %copy.28 = f32[2,32,16,2,128]{4,3,2,1,0:T(2,128)} copy(f32[2,32,16,2,128]{4,3,2,1,0:T(2,128)} %bitcast.24) | data formatting | bytes 2097152
  (2 shorter events, 0.0 us)
Async XLA Ops:
  0.6 5.8 %copy-start = (bf16[2,16,2,2048]{3,2,1,0:T(2,128)(2,1)S(1)}, bf16[2,16,2,2048]{3,2,1,0:T(2,128)(2,1)}, u32[]{:S(2)}) copy-start(bf16[2,16,2,2048]{3,2,1,0:T(2,128)(2,1)} %param.19) | copy-start | bytes 786436

commit v2 on v1

--- a/solution.py
+++ b/solution.py
@@ -32,9 +32,9 @@
 
 
 def kernel(
-    x_ref, gain_ref, wt_ref, floor_ref, og_ref, wo_ref, st_hbm,
-    xo_ref, so_hbm,
-    gx, gq, gg, gr, wt, wo, st, kq, xs, xres, x1b,
+    x_ref, gain_ref, wq_ref, wf_ref, wv_ref, wg_ref, floor_ref, og_ref, wo_ref, st_hbm,
+    xo_ref, st,
+    gx, gq, gg, gr, wt, wo, wsrc, own, kq, xs, xres, x1b, vt,
     sx, rx, sw, rw, so_s, so_r, lsem,
 ):
     tp = lax.axis_index("tp")
@@ -55,7 +55,8 @@
     bar = pltpu.get_barrier_semaphore()
     for p in zp + yp + dpp:
         pl.semaphore_signal(bar, inc=1, device_id=p, device_id_type=MESH)
-    gx[0, y, z, 0] = x_ref[...]
+    x_in = x_ref[...].astype(F32)
+    gx[0, y, z, 0] = jnp.concatenate([x_in[8 * a : 8 * a + 8] for a in range(4)], axis=1).astype(BF16)
     pl.semaphore_wait(bar, len(zp) + len(yp) + len(dpp))
 
     def send(src, dst, s, r, p):
@@ -87,13 +88,27 @@
 
     z_send(gx.at[0], 0)
     for b in range(2):
+        own[b, 0:32, :] = wq_ref[b]
+        own[b, 32:64, :] = wf_ref[b]
+        own[b, 64:96, :] = wv_ref[b].reshape(32, 256)
+        own[b, 96:128, :] = wg_ref[b].reshape(32, 256)
+        wt[b, dp] = own[b]
         for p in dpp:
-            send(wt_ref.at[b], wt.at[b, dp], sw.at[b], rw.at[b], p)
+            send(own.at[b], wt.at[b, dp], sw.at[b], rw.at[b], p)
+    for k in range(NZ):
+        wsrc[k] = wo_ref[core, :, :, 128 * k : 128 * k + 128].reshape(32, 128)
+    wo[core, z, y] = wsrc[z]
     for i, p in zip(zi, zp):
-        send(wo_ref.at[core, i], wo.at[core, z, y], so_s.at[0], so_r.at[0], p)
+        send(wsrc.at[i], wo.at[core, z, y], so_s.at[0], so_r.at[0], p)
+    spot = lax.broadcasted_iota(jnp.int32, (16, 128), 1) % 32
+    head = lax.broadcasted_iota(jnp.int32, (16, 128), 0)
+    gains = []
     for b in range(2):
-        wt[b, dp] = wt_ref[b]
-    wo[core, z, y] = wo_ref[core, z]
+        row = jnp.zeros((1, 128), F32)
+        for j in range(2):
+            pick = jnp.where(spot == 2 * head + j, 1.0, 0.0)
+            row = row + jnp.dot(og_ref[b, j : j + 1, :], pick, precision=lax.Precision.HIGHEST, preferred_element_type=F32)
+        gains.append(row)
     z_wait(gx.at[0], 0)
     y_send(gx.at[0], 0)
     arrived(wt.at[0, pl.ds(0, NDP - 1)], sw.at[0], rw.at[0])
@@ -130,13 +145,13 @@
         gq[b, y, z, 1] = packed[1].astype(BF16)
         z_send(gq.at[b], base + 1)
         gate = packed[3]
-        gg[b, y, z, 0] = (og_ref[b : b + 1, :] * (gate / (1.0 + jnp.exp(-gate)))).astype(BF16)
+        gg[b, y, z, 0] = (gains[b] * (gate / (1.0 + jnp.exp(-gate)))).astype(BF16)
         z_send(gg.at[b], base + 2)
         if b == 0:
             arrived(wo.at[0, pl.ds(0, NZ - 1), 0], so_s.at[0], so_r.at[0])
             for p in yp:
                 send(wo.at[core, :, y], wo.at[core, :, y], so_s.at[1], so_r.at[1], p)
-        vt = jnp.transpose(jnp.concatenate([proj, jnp.zeros((96, 128), F32)], axis=0))
+        vt[...] = jnp.transpose(jnp.concatenate([proj, jnp.zeros((96, 128), F32)], axis=0))
         z_wait(gq.at[b], base + 1)
         y_send(gq.at[b], base + 1)
         z_wait(gg.at[b], base + 2)
@@ -153,6 +168,7 @@
         loads[b].wait()
         lane = lanes()
         read = [[jnp.zeros((8, 128), F32) for _ in range(2)] for _ in range(2)]
+        vals = [[vt[pl.ds(64 + 16 * hh + j, 8, stride=2), :] for hh in range(2)] for j in range(2)]
         for s in range(32):
             for hh in range(2):
                 keep = kq[0, s * PITCH + 8 * hh : s * PITCH + 8 * hh + 8, :]
@@ -160,34 +176,37 @@
                 rest = 1.0 - keep
                 for j in range(2):
                     rows = pl.ds(s * 32 + hh * 16 + j, 8, stride=2)
-                    row0 = 64 + j * 16 + hh * 8
-                    new = keep * st[b, rows, :] + rest * vt[row0 : row0 + 8, s : s + 1]
+                    new = keep * st[b, rows, :] + rest * vals[j][hh][:, s : s + 1]
                     st[b, rows, :] = new
                     red = jnp.sum(quer * new, axis=1, keepdims=True)
                     read[j][hh] = jnp.where(lane == s, red, read[j][hh])
-        rt = jnp.concatenate([read[0][0], read[0][1], read[1][0], read[1][1], jnp.zeros((96, 128), F32)], axis=0)
-        rt = jnp.transpose(rt)
+        vt[...] = jnp.zeros((128, 128), F32)
+        for j in range(2):
+            for hh in range(2):
+                vt[pl.ds(16 * hh + j, 8, stride=2), :] = read[j][hh]
+        rt = jnp.transpose(vt[...])
         tile = rt[0:8]
         for a in range(1, 4):
             tile = tile + pltpu.roll(rt[8 * a : 8 * a + 8], 32 * a, 1)
-        gr[b, y, z, 0] = tile.astype(BF16)
-        z_send(gr.at[b], base + 3)
-        store = pltpu.make_async_copy(st.at[b], so_hbm.at[b], lsem.at[2 + b])
-        store.start()
-        if b == 0:
-            first_store = store
+        gr[b, y * NZ + z] = tile.astype(BF16)
+        for i in zi:
+            for k in (2, 1, 3, 0):
+                to = {"tp": i * NY + lax.rem(y + k, NY)}
+                send(gr.at[b, y * NZ + z], gr.at[b, y * NZ + z], sx.at[base + 3, 0], rx.at[base + 3, 0], to)
+        for p in yp:
+            send(gr.at[b, y * NZ + z], gr.at[b, y * NZ + z], sx.at[base + 3, 0], rx.at[base + 3, 0], p)
+        if b == 0:
             arrived(wo.at[0, pl.ds(0, NZ), pl.ds(0, NY - 1)], so_s.at[1], so_r.at[1])
             send(wo.at[core], wo.at[core], so_s.at[2], so_r.at[2], mate)
         y_wait(gg.at[b], base + 2)
         gate = turn([gg[b, i, :, 0].astype(F32) for i in range(NY)])
-        z_wait(gr.at[b], base + 3)
-        y_send(gr.at[b], base + 3)
-        y_wait(gr.at[b], base + 3)
-        read = turn([gr[b, i, :, 0].astype(F32) for i in range(NY)])
+        arrived(gr.at[b, pl.ds(0, NY * NZ - 1)], sx.at[base + 3, 0], rx.at[base + 3, 0])
+        read = turn([gr[b, NZ * i : NZ * i + NZ].astype(F32) for i in range(NY)])
         for a in range(4):
             sq = jnp.sum(read[a] * read[a], axis=0)
-            for shift in (64, 32, 16):
+            for shift in (64, 32):
                 sq = sq + pltpu.roll(sq, shift, 1)
+            sq = sq + jnp.where(lane % 2 == 0, pltpu.roll(sq, 127, 1), pltpu.roll(sq, 1, 1))
             scale = lax.rsqrt(sq / 128.0 + EPS)
             for k in range(NZ):
                 xs[8 * a : 8 * a + 8, 128 * k : 128 * k + 128] = (read[a][k] * scale * gate[a][k]).astype(BF16)
@@ -215,57 +234,61 @@
         all_left(gx.at[b], 4 * b)
         all_left(gq.at[b], 4 * b + 1)
         all_left(gg.at[b], 4 * b + 2)
-        all_left(gr.at[b], 4 * b + 3)
+        left(gr.at[b, pl.ds(0, NY * NZ - 1)], sx.at[4 * b + 3, 0], rx.at[4 * b + 3, 0])
         left(wt.at[b, pl.ds(0, NDP - 1)], sw.at[b], rw.at[b])
     left(wo.at[0, pl.ds(0, NZ - 1), 0], so_s.at[0], so_r.at[0])
     left(wo.at[0, pl.ds(0, NZ), pl.ds(0, NY - 1)], so_s.at[1], so_r.at[1])
     left(wo.at[0], so_s.at[2], so_r.at[2])
-    first_store.wait()
-    store.wait()
 
 
 def shards(
     resid, norm_gain, w_query, w_forget, w_value, w_gate, gate_floor, states, out_gain, w_out
 ):
-    seqs = resid.shape[0]
-    x = resid.reshape(4, 8, 32).transpose(1, 0, 2).reshape(8, 128)
-    value_t = w_value.transpose(0, 3, 2, 1).reshape(2, 32, 256)
-    gate_t = w_gate.transpose(0, 3, 2, 1).reshape(2, 32, 256)
-    wt = jnp.concatenate([w_query.transpose(0, 2, 1), w_forget.transpose(0, 2, 1), value_t, gate_t], axis=1)
-    og = jnp.tile(out_gain.transpose(0, 2, 1).reshape(2, 32), (1, 4))
-    wo = w_out.transpose(0, 2, 1, 3).reshape(2, 32, 16, 128).transpose(0, 2, 1, 3)
-    st = states.reshape(2, seqs * 32, 128)
+    st = states.reshape(2, resid.shape[0] * 32, 128)
     vmem = pl.BlockSpec(memory_space=pltpu.VMEM)
     hbm = pl.BlockSpec(memory_space=pl.ANY)
     dma = pltpu.SemaphoreType.DMA
     new_resid, new_states = pl.pallas_call(
         kernel,
-        out_shape=(jax.ShapeDtypeStruct((32, 32), BF16), jax.ShapeDtypeStruct(st.shape, F32)),
-        in_specs=[vmem] * 6 + [hbm],
-        out_specs=(vmem, hbm),
+        out_shape=(pltpu.VMEM((32, 32), BF16), pltpu.VMEM(st.shape, F32)),
+        in_specs=[vmem] * 9 + [hbm],
+        out_specs=(vmem, vmem),
         scratch_shapes=[
             pltpu.VMEM((2, NY, NZ, 1, 8, 128), BF16),
             pltpu.VMEM((2, NY, NZ, 2, 8, 128), BF16),
             pltpu.VMEM((2, NY, NZ, 1, 8, 128), BF16),
-            pltpu.VMEM((2, NY, NZ, 1, 8, 128), BF16),
+            pltpu.VMEM((2, NY * NZ, 8, 128), BF16),
             pltpu.VMEM((2, NDP, 128, 256), BF16),
             pltpu.VMEM((2, NZ, NY, 32, 128), BF16),
-            pltpu.VMEM((2, 1024, 128), F32),
+            pltpu.VMEM((NZ, 32, 128), BF16),
+            pltpu.VMEM((2, 128, 256), BF16),
             pltpu.VMEM((2, 32 * PITCH, 128), F32),
             pltpu.VMEM((32, 2048), BF16),
             pltpu.VMEM((NZ, 32, 128), F32),
             pltpu.VMEM((4, 8, 128), BF16),
+            pltpu.VMEM((128, 128), F32),
             dma((8, 2)),
             dma((8, 2)),
             dma((2,)),
             dma((2,)),
             dma((3,)),
             dma((3,)),
-            dma((4,)),
+            dma((2,)),
         ],
         compiler_params=pltpu.CompilerParams(collective_id=0, has_side_effects=True),
         name="blocks",
-    )(x, norm_gain, wt, gate_floor, og, wo, st)
+    )(
+        resid,
+        norm_gain,
+        w_query.transpose(0, 2, 1),
+        w_forget.transpose(0, 2, 1),
+        w_value.transpose(0, 2, 3, 1),
+        w_gate.transpose(0, 2, 3, 1),
+        gate_floor,
+        out_gain.transpose(0, 2, 1),
+        w_out,
+        st,
+    )
     return new_resid, new_states.reshape(states.shape)
 
 

time: 103 us -> 89.1 us (0.87)
  local copies, waits for them, and re-layouts: 8.81 us -> 1.57 us
  Pallas kernels: 91.6 us -> 86.8 us
  other arithmetic: 1.43 us -> 0 us
    pallas_call x1, Pallas kernels: 91.6 us -> 86.8 us  [shards(): pl.pallas_call(kernel, out_shape=(pltpu.VMEM((32, 32), BF16), pltpu.VMEM(...]
    reshape x3 -> x0, local copies, waits for them, and re-layouts: 2.14 us -> none  [the longest x2 1.37 us: shards(): x = resid.reshape(4, 8, 32).transpose(1, 0, 2).reshape(8, 128)]
    unnamed x5 -> x2, local copies, waits for them, and re-layouts: 3.6 us -> 1.57 us
    transpose x3 -> x0, local copies, waits for them, and re-layouts: 1.61 us -> none  [the longest x1 0.76 us: shards(): value_t = w_value.transpose(0, 3, 2, 1).reshape(2, 32, 256)]
    another operation x3 -> x0, local copies, waits for them, and re-layouts: 1.47 us -> none  [shards(): og = jnp.tile(out_gain.transpose(0, 2, 1).reshape(2, 32), (1, 4))]
    concatenate x1 -> x0, other arithmetic: 1.43 us -> none  [shards(): jnp.concatenate([w_query.transpose(0, 2, 1), w_forget.transpose(0, 2, 1),...]
where the time goes in v2:
time: 89.1 us; the launch traced here: 89 us
  Pallas kernels  86.8 us (97%)
  local copies, waits for them, and re-layouts  1.57 us (2%)
    pallas_call x1, Pallas kernels, shards(): pl.pallas_call(kernel, out_shape=(pltpu.VMEM((32, 32), BF16), pltpu.VMEM(...  86.8 us

profile of v2, /device:TPU:6, one launch (start us, length us, event | category | flops | bytes accessed | tf_op | source)
XLA Modules:
  0.0 89.0 jit_solution(15294331122710393279)
XLA Ops:
  0.6 86.8 %blocks.1 = (bf16[32,32]{1,0:T(8,128)(2,1)S(1)}, f32[2,1024,128]{2,1,0:T(8,128)S(1)}) custom-call(bf16[32,32]{1,0:T(8,128)(2,1)} %x_ref.1, f32[2,2048]{1,0:T(2,128)} %gain_ref.1, bf16[2,32,256]{2,1,0:T(8,128)(2,1)} %bitcast.9, bf16[2,32,256]{2,1,0:T(8,128)(2,1)} %bitcast.10, bf16[2,16,2,256]{3,2,1,0:T(2,128)(2,1)} %bitcast.11, ...), custom_call_target="tpu_custom_call" | custom-call | tf_op jit(solution)/shard_map/blocks/pallas_call | solution.py:251
  87.4 0.6 copy.14
  88.0 1.0 %copy.15 = f32[2,32,16,2,128]{4,3,2,1,0:T(2,128)} copy(f32[2,32,16,2,128]{4,3,2,1,0:T(2,128)S(1)} %bitcast.7) | data formatting | bytes 2097152

commit v3 on v2

--- a/solution.py
+++ b/solution.py
@@ -34,7 +34,7 @@
 def kernel(
     x_ref, gain_ref, wq_ref, wf_ref, wv_ref, wg_ref, floor_ref, og_ref, wo_ref, st_hbm,
     xo_ref, st,
-    gx, gq, gg, gr, wt, wo, wsrc, own, kq, xs, xres, x1b, vt,
+    x0, x1, gq, gg, gr, wt, wo, wsrc, own, kq, xs, xres, x1b, vt,
     sx, rx, sw, rw, so_s, so_r, lsem,
 ):
     tp = lax.axis_index("tp")
@@ -42,6 +42,7 @@
     z, y = tp // NY, tp % NY
     core = dp % 2
     zdist = (8, 7, 9, 6, 10, 5, 11, 4, 12, 3, 13, 2, 14, 1, 15)
+    zclose = (4, -4, 3, -3, 2, -2, 1, -1)
     zi = [lax.rem(z + k, NZ) for k in zdist]
     zp = [{"tp": i * NY + y} for i in zi]
     yp = [{"tp": z * NY + lax.rem(y + k, NY)} for k in (2, 1, 3)]
@@ -53,11 +54,12 @@
         c.start()
 
     bar = pltpu.get_barrier_semaphore()
-    for p in zp + yp + dpp:
+    zc = [{"tp": lax.rem(z + NZ + k, NZ) * NY + y} for k in zclose]
+    for p in zc + yp + dpp:
         pl.semaphore_signal(bar, inc=1, device_id=p, device_id_type=MESH)
     x_in = x_ref[...].astype(F32)
-    gx[0, y, z, 0] = jnp.concatenate([x_in[8 * a : 8 * a + 8] for a in range(4)], axis=1).astype(BF16)
-    pl.semaphore_wait(bar, len(zp) + len(yp) + len(dpp))
+    x0[y, 8] = jnp.concatenate([x_in[8 * a : 8 * a + 8] for a in range(4)], axis=1).astype(BF16)
+    pl.semaphore_wait(bar, len(zc) + len(yp) + len(dpp))
 
     def send(src, dst, s, r, p):
         pltpu.make_async_remote_copy(src, dst, s, r, device_id=p, device_id_type=MESH).start()
@@ -82,11 +84,23 @@
     def y_wait(buf, i):
         arrived(buf.at[pl.ds(0, NY - 1)], sx.at[i, 1], rx.at[i, 1])
 
+    def to_all(buf, i):
+        tile = buf.at[y * NZ + z]
+        for j in zi:
+            for k in (2, 1, 3, 0):
+                send(tile, tile, sx.at[i, 0], rx.at[i, 0], {"tp": j * NY + lax.rem(y + k, NY)})
+        for p in yp:
+            send(tile, tile, sx.at[i, 0], rx.at[i, 0], p)
+
+    def all_here(buf, i):
+        arrived(buf.at[pl.ds(0, NY * NZ - 1)], sx.at[i, 0], rx.at[i, 0])
+
     def all_left(buf, i):
         left(buf.at[0, pl.ds(0, NZ - 1)], sx.at[i, 0], rx.at[i, 0])
         left(buf.at[pl.ds(0, NY - 1)], sx.at[i, 1], rx.at[i, 1])
 
-    z_send(gx.at[0], 0)
+    for k, p in zip(zclose, zc):
+        send(x0.at[y, 8], x0.at[y, 8 - k], sx.at[0, 0], rx.at[0, 0], p)
     for b in range(2):
         own[b, 0:32, :] = wq_ref[b]
         own[b, 32:64, :] = wf_ref[b]
@@ -98,8 +112,6 @@
     for k in range(NZ):
         wsrc[k] = wo_ref[core, :, :, 128 * k : 128 * k + 128].reshape(32, 128)
     wo[core, z, y] = wsrc[z]
-    for i, p in zip(zi, zp):
-        send(wsrc.at[i], wo.at[core, z, y], so_s.at[0], so_r.at[0], p)
     spot = lax.broadcasted_iota(jnp.int32, (16, 128), 1) % 32
     head = lax.broadcasted_iota(jnp.int32, (16, 128), 0)
     gains = []
@@ -109,20 +121,33 @@
             pick = jnp.where(spot == 2 * head + j, 1.0, 0.0)
             row = row + jnp.dot(og_ref[b, j : j + 1, :], pick, precision=lax.Precision.HIGHEST, preferred_element_type=F32)
         gains.append(row)
-    z_wait(gx.at[0], 0)
-    y_send(gx.at[0], 0)
+    arrived(x0.at[0, pl.ds(0, 8)], sx.at[0, 0], rx.at[0, 0])
+    for k in (2, 1, 3, 0):
+        yk = lax.rem(y + k, NY)
+        up = {"tp": lax.rem(z + 4, NZ) * NY + yk}
+        down = {"tp": lax.rem(z + NZ - 4, NZ) * NY + yk}
+        send(x0.at[y, pl.ds(4, 4)], x0.at[y, pl.ds(0, 4)], sx.at[0, 1], rx.at[0, 1], up)
+        send(x0.at[y, pl.ds(9, 3)], x0.at[y, pl.ds(13, 3)], sx.at[0, 1], rx.at[0, 1], down)
+    for p in yp:
+        send(x0.at[y, pl.ds(4, 9)], x0.at[y, pl.ds(4, 9)], sx.at[0, 1], rx.at[0, 1], p)
+    for i, p in zip(zi, zp):
+        send(wsrc.at[i], wo.at[core, z, y], so_s.at[0], so_r.at[0], p)
     arrived(wt.at[0, pl.ds(0, NDP - 1)], sw.at[0], rw.at[0])
-    y_wait(gx.at[0], 0)
+    arrived(gr.at[0, pl.ds(0, 55)], sx.at[0, 1], rx.at[0, 1])
 
     for b in range(2):
         base = 4 * b
         if b == 0:
-            tiles = turn([gx[0, i, :, 0].astype(F32) for i in range(NY)])
-            for a in range(4):
-                for k in range(NZ):
-                    xres[k, 8 * a : 8 * a + 8, :] = tiles[a][k]
+            tiles = [[], [], [], []]
+            for k in range(NZ):
+                slot = lax.rem(k + 24 - z, NZ)
+                four = turn([x0[i, slot].astype(F32) for i in range(NY)])
+                for a in range(4):
+                    tiles[a].append(four[a])
+                    xres[k, 8 * a : 8 * a + 8, :] = four[a]
+            tiles = [jnp.stack(t) for t in tiles]
         else:
-            tiles = [gx[1, a, :, 0].astype(F32) for a in range(NY)]
+            tiles = [x1[NZ * a : NZ * a + NZ].astype(F32) for a in range(NY)]
         inv = []
         for a in range(4):
             sq = jnp.sum(jnp.sum(tiles[a] * tiles[a], axis=0), axis=1, keepdims=True)
@@ -189,18 +214,13 @@
         for a in range(1, 4):
             tile = tile + pltpu.roll(rt[8 * a : 8 * a + 8], 32 * a, 1)
         gr[b, y * NZ + z] = tile.astype(BF16)
-        for i in zi:
-            for k in (2, 1, 3, 0):
-                to = {"tp": i * NY + lax.rem(y + k, NY)}
-                send(gr.at[b, y * NZ + z], gr.at[b, y * NZ + z], sx.at[base + 3, 0], rx.at[base + 3, 0], to)
-        for p in yp:
-            send(gr.at[b, y * NZ + z], gr.at[b, y * NZ + z], sx.at[base + 3, 0], rx.at[base + 3, 0], p)
+        to_all(gr.at[b], base + 3)
         if b == 0:
             arrived(wo.at[0, pl.ds(0, NZ), pl.ds(0, NY - 1)], so_s.at[1], so_r.at[1])
             send(wo.at[core], wo.at[core], so_s.at[2], so_r.at[2], mate)
         y_wait(gg.at[b], base + 2)
         gate = turn([gg[b, i, :, 0].astype(F32) for i in range(NY)])
-        arrived(gr.at[b, pl.ds(0, NY * NZ - 1)], sx.at[base + 3, 0], rx.at[base + 3, 0])
+        all_here(gr.at[b], base + 3)
         read = turn([gr[b, NZ * i : NZ * i + NZ].astype(F32) for i in range(NY)])
         for a in range(4):
             sq = jnp.sum(read[a] * read[a], axis=0)
@@ -218,11 +238,9 @@
             xres[0] = fresh
             for a in range(4):
                 x1b[a] = fresh[8 * a : 8 * a + 8].astype(BF16)
-            gx[1, y, z, 0] = x1b[y]
-            z_send(gx.at[1], 4)
-            z_wait(gx.at[1], 4)
-            y_send(gx.at[1], 4)
-            y_wait(gx.at[1], 4)
+            x1[y * NZ + z] = x1b[y]
+            to_all(x1, 4)
+            all_here(x1, 4)
         else:
             fresh = xres[0] + branch
             mine = fresh
@@ -231,11 +249,13 @@
             xo_ref[...] = mine[:, :32].astype(BF16)
 
     for b in range(2):
-        all_left(gx.at[b], 4 * b)
         all_left(gq.at[b], 4 * b + 1)
         all_left(gg.at[b], 4 * b + 2)
         left(gr.at[b, pl.ds(0, NY * NZ - 1)], sx.at[4 * b + 3, 0], rx.at[4 * b + 3, 0])
         left(wt.at[b, pl.ds(0, NDP - 1)], sw.at[b], rw.at[b])
+    left(x0.at[0, pl.ds(0, 8)], sx.at[0, 0], rx.at[0, 0])
+    left(gr.at[0, pl.ds(0, 55)], sx.at[0, 1], rx.at[0, 1])
+    left(x1.at[pl.ds(0, NY * NZ - 1)], sx.at[4, 0], rx.at[4, 0])
     left(wo.at[0, pl.ds(0, NZ - 1), 0], so_s.at[0], so_r.at[0])
     left(wo.at[0, pl.ds(0, NZ), pl.ds(0, NY - 1)], so_s.at[1], so_r.at[1])
     left(wo.at[0], so_s.at[2], so_r.at[2])
@@ -254,7 +274,8 @@
         in_specs=[vmem] * 9 + [hbm],
         out_specs=(vmem, vmem),
         scratch_shapes=[
-            pltpu.VMEM((2, NY, NZ, 1, 8, 128), BF16),
+            pltpu.VMEM((NY, NZ, 8, 128), BF16),
+            pltpu.VMEM((NY * NZ, 8, 128), BF16),
             pltpu.VMEM((2, NY, NZ, 2, 8, 128), BF16),
             pltpu.VMEM((2, NY, NZ, 1, 8, 128), BF16),
             pltpu.VMEM((2, NY * NZ, 8, 128), BF16),

time: 89.1 us -> 84.3 us (0.946); the launches traced: 89 us -> 83.2 us
  Pallas kernels: 86.8 us -> 81 us
    pallas_call x1, Pallas kernels: 86.8 us -> 81 us  [shards(): pl.pallas_call(kernel, out_shape=(pltpu.VMEM((32, 32), BF16), pltpu.VMEM(...]
where the time goes in v3:
time: 84.3 us; the launch traced here: 83.2 us
  Pallas kernels  81 us (96%)
  local copies, waits for them, and re-layouts  1.57 us (2%)
    pallas_call x1, Pallas kernels, shards(): pl.pallas_call(kernel, out_shape=(pltpu.VMEM((32, 32), BF16), pltpu.VMEM(...  81 us

profile of v3, /device:TPU:6, one launch (start us, length us, event | category | flops | bytes accessed | tf_op | source)
XLA Modules:
  0.0 83.2 jit_solution(16038123667874463217)
XLA Ops:
  0.6 81.0 %blocks.1 = (bf16[32,32]{1,0:T(8,128)(2,1)S(1)}, f32[2,1024,128]{2,1,0:T(8,128)S(1)}) custom-call(bf16[32,32]{1,0:T(8,128)(2,1)} %x_ref.1, f32[2,2048]{1,0:T(2,128)} %gain_ref.1, bf16[2,32,256]{2,1,0:T(8,128)(2,1)} %bitcast.9, bf16[2,32,256]{2,1,0:T(8,128)(2,1)} %bitcast.10, bf16[2,16,2,256]{3,2,1,0:T(2,128)(2,1)} %bitcast.11, ...), custom_call_target="tpu_custom_call" | custom-call | tf_op jit(solution)/shard_map/blocks/pallas_call | solution.py:271
  81.6 0.6 copy.14
  82.2 1.0 %copy.15 = f32[2,32,16,2,128]{4,3,2,1,0:T(2,128)} copy(f32[2,32,16,2,128]{4,3,2,1,0:T(2,128)S(1)} %bitcast.7) | data formatting | bytes 2097152

commit v4 on v3

--- a/solution.py
+++ b/solution.py
@@ -34,7 +34,7 @@
 def kernel(
     x_ref, gain_ref, wq_ref, wf_ref, wv_ref, wg_ref, floor_ref, og_ref, wo_ref, st_hbm,
     xo_ref, st,
-    x0, x1, gq, gg, gr, wt, wo, wsrc, own, kq, xs, xres, x1b, vt,
+    x0, x1, gq, gq1, gg, gr, wt, wide, wq1, wv1, wo, wsrc, own, kq, xs, xres, x1b, vt,
     sx, rx, sw, rw, so_s, so_r, lsem,
 ):
     tp = lax.axis_index("tp")
@@ -48,6 +48,9 @@
     yp = [{"tp": z * NY + lax.rem(y + k, NY)} for k in (2, 1, 3)]
     dpp = [{"dp": lax.rem(dp + k, NDP)} for k in (4, 3, 5, 2, 6, 1, 7)]
     mate = {"dp": dp + 1 - 2 * core}
+    x = dp // 2
+    xp = [{"dp": lax.rem(x + k, 4) * 2 + core} for k in (2, 1, 3)]
+    cls, turnover = z % 4, z // 4
 
     loads = [pltpu.make_async_copy(st_hbm.at[b], st.at[b], lsem.at[b]) for b in range(2)]
     for c in loads:
@@ -106,12 +109,15 @@
         own[b, 32:64, :] = wf_ref[b]
         own[b, 64:96, :] = wv_ref[b].reshape(32, 256)
         own[b, 96:128, :] = wg_ref[b].reshape(32, 256)
-        wt[b, dp] = own[b]
-        for p in dpp:
-            send(own.at[b], wt.at[b, dp], sw.at[b], rw.at[b], p)
+        if b == 0:
+            wt[dp] = own[0]
+            for p in dpp:
+                send(own.at[0], wt.at[dp], sw.at[0], rw.at[0], p)
+    wide[turnover] = own[1, 0:64, :]
+    wv1[x, core] = own[1, 64:128, :]
     for k in range(NZ):
-        wsrc[k] = wo_ref[core, :, :, 128 * k : 128 * k + 128].reshape(32, 128)
-    wo[core, z, y] = wsrc[z]
+        wsrc[k] = wo_ref[core, :, :, 128 * k : 128 * k + 128].reshape(4, 8, 128)
+    wo[core, z, y, x] = wsrc[z, x]
     spot = lax.broadcasted_iota(jnp.int32, (16, 128), 1) % 32
     head = lax.broadcasted_iota(jnp.int32, (16, 128), 0)
     gains = []
@@ -131,9 +137,18 @@
     for p in yp:
         send(x0.at[y, pl.ds(4, 9)], x0.at[y, pl.ds(4, 9)], sx.at[0, 1], rx.at[0, 1], p)
     for i, p in zip(zi, zp):
-        send(wsrc.at[i], wo.at[core, z, y], so_s.at[0], so_r.at[0], p)
-    arrived(wt.at[0, pl.ds(0, NDP - 1)], sw.at[0], rw.at[0])
+        send(wsrc.at[i, x], wo.at[core, z, y, x], so_s.at[0], so_r.at[0], p)
+    arrived(wt.at[pl.ds(0, NDP - 1)], sw.at[0], rw.at[0])
     arrived(gr.at[0, pl.ds(0, 55)], sx.at[0, 1], rx.at[0, 1])
+
+    def project(weights, width, inv):
+        total = jnp.zeros((32, width), F32)
+        for d in range(NDP):
+            part = lax.dot_general(
+                xs[:, 256 * d : 256 * d + 256], weights(d), (((1,), (1,)), ((), ())), preferred_element_type=F32
+            )
+            total = total + part.astype(BF16).astype(F32)
+        return (total * inv).astype(BF16).astype(F32)
 
     for b in range(2):
         base = 4 * b
@@ -156,44 +171,69 @@
                 scaled = tiles[a][k] * gain_ref[b : b + 1, 128 * k : 128 * k + 128]
                 xs[8 * a : 8 * a + 8, 128 * k : 128 * k + 128] = scaled.astype(BF16)
         inv = jnp.concatenate(inv, axis=0)
+        if b == 0:
+            proj = project(lambda d: wt[d], 128, inv)
+            packed = turn([proj[8 * a : 8 * a + 8] for a in range(4)])
+            gq[y, z, 0] = packed[0].astype(BF16)
+            gq[y, z, 1] = packed[1].astype(BF16)
+            z_send(gq, 1)
+            gate = packed[3]
+        else:
+            arrived(wq1.at[:, 0], sw.at[4], rw.at[4])
+            arrived(wv1.at[:, 0], sw.at[5], rw.at[5])
+            proj = project(lambda d: wq1[d // 2, d % 2].reshape(256, 256), 256, inv)
+            unit = (y * 4 + cls) * 4
+            for half in range(2):
+                packed = turn([proj[8 * a : 8 * a + 8, 128 * half : 128 * half + 128] for a in range(4)])
+                for q in range(2):
+                    gq1[unit + 2 * half + q, 0] = packed[2 * q].astype(BF16)
+                    gq1[unit + 2 * half + q, 1] = packed[2 * q + 1].astype(BF16)
+            for k, first, count in ((2, 2, 2), (-2, 0, 2), (1, 0, 4), (-1, 0, 4), (0, 0, 4)):
+                for j in (2, 1, 3) if k == 0 else (2, 1, 3, 0):
+                    to = {"tp": lax.rem(z + NZ + k, NZ) * NY + lax.rem(y + j, NY)}
+                    part = gq1.at[pl.ds(unit + first, count)]
+                    send(part, part, sx.at[5, 0], rx.at[5, 0], to)
+            proj = jnp.concatenate([project(lambda d: wv1[d // 2, d % 2], 64, inv), jnp.zeros((32, 64), F32)], axis=1)
+            gate = turn([proj[8 * a : 8 * a + 8] for a in range(4)])[1]
+        gg[b, y, z, 0] = (gains[b] * (gate / (1.0 + jnp.exp(-gate)))).astype(BF16)
         if b == 1:
-            arrived(wt.at[1, pl.ds(0, NDP - 1)], sw.at[1], rw.at[1])
-        total = jnp.zeros((32, 128), F32)
-        for d in range(NDP):
-            part = lax.dot_general(
-                xs[:, 256 * d : 256 * d + 256], wt[b, d], (((1,), (1,)), ((), ())), preferred_element_type=F32
-            )
-            total = total + part.astype(BF16).astype(F32)
-        proj = (total * inv).astype(BF16).astype(F32)
-        packed = turn([proj[8 * a : 8 * a + 8] for a in range(4)])
-        gq[b, y, z, 0] = packed[0].astype(BF16)
-        gq[b, y, z, 1] = packed[1].astype(BF16)
-        z_send(gq.at[b], base + 1)
-        gate = packed[3]
-        gg[b, y, z, 0] = (gains[b] * (gate / (1.0 + jnp.exp(-gate)))).astype(BF16)
-        z_send(gg.at[b], base + 2)
-        if b == 0:
-            arrived(wo.at[0, pl.ds(0, NZ - 1), 0], so_s.at[0], so_r.at[0])
+            z_send(gg.at[b], base + 2)
+        else:
+            arrived(gr.at[0, pl.ds(0, NZ - 1)], so_s.at[0], so_r.at[0])
             for p in yp:
-                send(wo.at[core, :, y], wo.at[core, :, y], so_s.at[1], so_r.at[1], p)
+                send(wo.at[core, :, y, x], wo.at[core, :, y, x], so_s.at[1], so_r.at[1], p)
         vt[...] = jnp.transpose(jnp.concatenate([proj, jnp.zeros((96, 128), F32)], axis=0))
-        z_wait(gq.at[b], base + 1)
-        y_send(gq.at[b], base + 1)
-        z_wait(gg.at[b], base + 2)
-        y_send(gg.at[b], base + 2)
-        y_wait(gq.at[b], base + 1)
-        forget = turn([gq[b, i, :, 1].astype(F32) for i in range(NY)])
-        query = turn([gq[b, i, :, 0].astype(F32) for i in range(NY)])
-        for a in range(4):
-            for k in range(NZ):
-                low = floor_ref[b : b + 1, 128 * k : 128 * k + 128]
-                keep = low + (1.0 - low) * (1.0 / (1.0 + jnp.exp(-forget[a][k])))
-                kq[0, pl.ds(8 * a * PITCH + k, 8, stride=PITCH), :] = keep
-                kq[1, pl.ds(8 * a * PITCH + k, 8, stride=PITCH), :] = query[a][k]
+        if b == 0:
+            z_wait(gq, 1)
+            y_send(gq, 1)
+            z_send(gg.at[0], 2)
+            for k in (8, 4, 12):
+                to = {"tp": lax.rem(z + k, NZ) * NY + y}
+                send(own.at[1, pl.ds(0, 64)], wide.at[turnover], sw.at[1], rw.at[1], to)
+            arrived(gr.at[0, pl.ds(0, 48)], so_s.at[1], so_r.at[1])
+            for p in xp:
+                send(wo.at[core, :, :, x], wo.at[core, :, :, x], so_s.at[2], so_r.at[2], p)
+            y_wait(gq, 1)
+        else:
+            arrived(gq1.at[pl.ds(0, 60)], sx.at[5, 0], rx.at[5, 0])
+        for k in range(NZ):
+            low = floor_ref[b : b + 1, 128 * k : 128 * k + 128]
+            for p in range(2):
+                if b == 0:
+                    four = turn([gq[i, k, p].astype(F32) for i in range(NY)])
+                else:
+                    four = turn([gq1[(4 * i + k % 4) * 4 + k // 4, p].astype(F32) for i in range(NY)])
+                for a in range(4):
+                    rows = pl.ds(8 * a * PITCH + k, 8, stride=PITCH)
+                    if p == 0:
+                        kq[1, rows, :] = four[a]
+                    else:
+                        kq[0, rows, :] = low + (1.0 - low) * (1.0 / (1.0 + jnp.exp(-four[a])))
         loads[b].wait()
         lane = lanes()
         read = [[jnp.zeros((8, 128), F32) for _ in range(2)] for _ in range(2)]
-        vals = [[vt[pl.ds(64 + 16 * hh + j, 8, stride=2), :] for hh in range(2)] for j in range(2)]
+        first = 64 if b == 0 else 0
+        vals = [[vt[pl.ds(first + 16 * hh + j, 8, stride=2), :] for hh in range(2)] for j in range(2)]
         for s in range(32):
             for hh in range(2):
                 keep = kq[0, s * PITCH + 8 * hh : s * PITCH + 8 * hh + 8, :]
@@ -216,8 +256,18 @@
         gr[b, y * NZ + z] = tile.astype(BF16)
         to_all(gr.at[b], base + 3)
         if b == 0:
-            arrived(wo.at[0, pl.ds(0, NZ), pl.ds(0, NY - 1)], so_s.at[1], so_r.at[1])
-            send(wo.at[core], wo.at[core], so_s.at[2], so_r.at[2], mate)
+            z_wait(gg.at[0], 2)
+            y_send(gg.at[0], 2)
+            arrived(wo.at[0, pl.ds(0, 12)], so_s.at[2], so_r.at[2])
+            send(wo.at[core], wo.at[core], so_s.at[3], so_r.at[3], mate)
+            arrived(wide.at[pl.ds(0, 3)], sw.at[1], rw.at[1])
+            for p in xp:
+                send(wide, wq1.at[x, core], sw.at[2], rw.at[2], p)
+                send(own.at[1, pl.ds(64, 64)], wv1.at[x, core], sw.at[3], rw.at[3], p)
+            wq1[x, core] = wide[...]
+        else:
+            z_wait(gg.at[1], 6)
+            y_send(gg.at[1], 6)
         y_wait(gg.at[b], base + 2)
         gate = turn([gg[b, i, :, 0].astype(F32) for i in range(NY)])
         all_here(gr.at[b], base + 3)
@@ -231,7 +281,7 @@
             for k in range(NZ):
                 xs[8 * a : 8 * a + 8, 128 * k : 128 * k + 128] = (read[a][k] * scale * gate[a][k]).astype(BF16)
         if b == 0:
-            arrived(wo.at[0], so_s.at[2], so_r.at[2])
+            arrived(wo.at[0], so_s.at[3], so_r.at[3])
         branch = jnp.dot(xs[...], wo[b].reshape(2048, 128), preferred_element_type=F32)
         if b == 0:
             fresh = (xres[z] + branch).astype(BF16).astype(F32)
@@ -240,6 +290,10 @@
                 x1b[a] = fresh[8 * a : 8 * a + 8].astype(BF16)
             x1[y * NZ + z] = x1b[y]
             to_all(x1, 4)
+            arrived(wq1.at[pl.ds(0, 3), 0], sw.at[2], rw.at[2])
+            arrived(wv1.at[pl.ds(0, 3), 0], sw.at[3], rw.at[3])
+            send(wq1.at[:, core], wq1.at[:, core], sw.at[4], rw.at[4], mate)
+            send(wv1.at[:, core], wv1.at[:, core], sw.at[5], rw.at[5], mate)
             all_here(x1, 4)
         else:
             fresh = xres[0] + branch
@@ -249,16 +303,23 @@
             xo_ref[...] = mine[:, :32].astype(BF16)
 
     for b in range(2):
-        all_left(gq.at[b], 4 * b + 1)
         all_left(gg.at[b], 4 * b + 2)
         left(gr.at[b, pl.ds(0, NY * NZ - 1)], sx.at[4 * b + 3, 0], rx.at[4 * b + 3, 0])
-        left(wt.at[b, pl.ds(0, NDP - 1)], sw.at[b], rw.at[b])
+    all_left(gq, 1)
+    left(gq1.at[pl.ds(0, 60)], sx.at[5, 0], rx.at[5, 0])
     left(x0.at[0, pl.ds(0, 8)], sx.at[0, 0], rx.at[0, 0])
     left(gr.at[0, pl.ds(0, 55)], sx.at[0, 1], rx.at[0, 1])
     left(x1.at[pl.ds(0, NY * NZ - 1)], sx.at[4, 0], rx.at[4, 0])
-    left(wo.at[0, pl.ds(0, NZ - 1), 0], so_s.at[0], so_r.at[0])
-    left(wo.at[0, pl.ds(0, NZ), pl.ds(0, NY - 1)], so_s.at[1], so_r.at[1])
-    left(wo.at[0], so_s.at[2], so_r.at[2])
+    left(wt.at[pl.ds(0, NDP - 1)], sw.at[0], rw.at[0])
+    left(wide.at[pl.ds(0, 3)], sw.at[1], rw.at[1])
+    left(wq1.at[pl.ds(0, 3), 0], sw.at[2], rw.at[2])
+    left(wv1.at[pl.ds(0, 3), 0], sw.at[3], rw.at[3])
+    left(wq1.at[:, 0], sw.at[4], rw.at[4])
+    left(wv1.at[:, 0], sw.at[5], rw.at[5])
+    left(gr.at[0, pl.ds(0, NZ - 1)], so_s.at[0], so_r.at[0])
+    left(gr.at[0, pl.ds(0, 48)], so_s.at[1], so_r.at[1])
+    left(wo.at[0, pl.ds(0, 12)], so_s.at[2], so_r.at[2])
+    left(wo.at[0], so_s.at[3], so_r.at[3])
 
 
 def shards(
@@ -276,12 +337,16 @@
         scratch_shapes=[
             pltpu.VMEM((NY, NZ, 8, 128), BF16),
             pltpu.VMEM((NY * NZ, 8, 128), BF16),
-            pltpu.VMEM((2, NY, NZ, 2, 8, 128), BF16),
+            pltpu.VMEM((NY, NZ, 2, 8, 128), BF16),
+            pltpu.VMEM((NY * NZ, 2, 8, 128), BF16),
             pltpu.VMEM((2, NY, NZ, 1, 8, 128), BF16),
             pltpu.VMEM((2, NY * NZ, 8, 128), BF16),
-            pltpu.VMEM((2, NDP, 128, 256), BF16),
-            pltpu.VMEM((2, NZ, NY, 32, 128), BF16),
-            pltpu.VMEM((NZ, 32, 128), BF16),
+            pltpu.VMEM((NDP, 128, 256), BF16),
+            pltpu.VMEM((4, 64, 256), BF16),
+            pltpu.VMEM((4, 2, 4, 64, 256), BF16),
+            pltpu.VMEM((4, 2, 64, 256), BF16),
+            pltpu.VMEM((2, NZ, NY, 4, 8, 128), BF16),
+            pltpu.VMEM((NZ, 4, 8, 128), BF16),
             pltpu.VMEM((2, 128, 256), BF16),
             pltpu.VMEM((2, 32 * PITCH, 128), F32),
             pltpu.VMEM((32, 2048), BF16),
@@ -290,10 +355,10 @@
             pltpu.VMEM((128, 128), F32),
             dma((8, 2)),
             dma((8, 2)),
-            dma((2,)),
-            dma((2,)),
-            dma((3,)),
-            dma((3,)),
+            dma((6,)),
+            dma((6,)),
+            dma((4,)),
+            dma((4,)),
             dma((2,)),
         ],
         compiler_params=pltpu.CompilerParams(collective_id=0, has_side_effects=True),

time: 84.3 us -> 77.7 us (0.922); the launches traced: 83.2 us -> 77.5 us
  Pallas kernels: 81 us -> 75.3 us
    pallas_call x1, Pallas kernels: 81 us -> 75.3 us  [shards(): pl.pallas_call(kernel, out_shape=(pltpu.VMEM((32, 32), BF16), pltpu.VMEM(...]
where the time goes in v4:
time: 77.7 us; the launch traced here: 77.5 us
  Pallas kernels  75.3 us (97%)
  local copies, waits for them, and re-layouts  1.57 us (2%)
    pallas_call x1, Pallas kernels, shards(): pl.pallas_call(kernel, out_shape=(pltpu.VMEM((32, 32), BF16), pltpu.VMEM(...  75.3 us
    unnamed x2, local copies, waits for them, and re-layouts  1.57 us

profile of v4, /device:TPU:6, one launch (start us, length us, event | category | flops | bytes accessed | tf_op | source)
XLA Modules:
  0.0 77.5 jit_solution(7902689661332022124)
XLA Ops:
  0.6 75.3 %blocks.1 = (bf16[32,32]{1,0:T(8,128)(2,1)S(1)}, f32[2,1024,128]{2,1,0:T(8,128)S(1)}) custom-call(bf16[32,32]{1,0:T(8,128)(2,1)} %x_ref.1, f32[2,2048]{1,0:T(2,128)} %gain_ref.1, bf16[2,32,256]{2,1,0:T(8,128)(2,1)} %bitcast.9, bf16[2,32,256]{2,1,0:T(8,128)(2,1)} %bitcast.10, bf16[2,16,2,256]{3,2,1,0:T(2,128)(2,1)} %bitcast.11, ...), custom_call_target="tpu_custom_call" | custom-call | tf_op jit(solution)/shard_map/blocks/pallas_call | solution.py:332
  75.9 0.6 copy.14
  76.5 1.0 %copy.15 = f32[2,32,16,2,128]{4,3,2,1,0:T(2,128)} copy(f32[2,32,16,2,128]{4,3,2,1,0:T(2,128)S(1)} %bitcast.7) | data formatting | bytes 2097152

commit v5 on v4

--- a/solution.py
+++ b/solution.py
@@ -32,9 +32,10 @@
 
 
 def kernel(
-    x_ref, gain_ref, wq_ref, wf_ref, wv_ref, wg_ref, floor_ref, og_ref, wo_ref, st_hbm,
+    x_hbm, gain_hbm, wq_hbm, wf_hbm, wv_hbm, wg_hbm, floor_hbm, og_hbm, wo_hbm, st_hbm,
     xo_ref, st,
     x0, x1, gq, gq1, gg, gr, wt, wide, wq1, wv1, wo, wsrc, own, kq, xs, xres, x1b, vt,
+    x_ref, gain_ref, wv_ref, wg_ref, floor_ref, og_ref, wo_ref,
     sx, rx, sw, rw, so_s, so_r, lsem,
 ):
     tp = lax.axis_index("tp")
@@ -52,14 +53,30 @@
     xp = [{"dp": lax.rem(x + k, 4) * 2 + core} for k in (2, 1, 3)]
     cls, turnover = z % 4, z // 4
 
-    loads = [pltpu.make_async_copy(st_hbm.at[b], st.at[b], lsem.at[b]) for b in range(2)]
-    for c in loads:
-        c.start()
-
     bar = pltpu.get_barrier_semaphore()
     zc = [{"tp": lax.rem(z + NZ + k, NZ) * NY + y} for k in zclose]
     for p in zc + yp + dpp:
         pl.semaphore_signal(bar, inc=1, device_id=p, device_id_type=MESH)
+    def load(src, dst, i):
+        copy = pltpu.make_async_copy(src, dst, lsem.at[i])
+        copy.start()
+        return copy
+
+    x_load = load(x_hbm, x_ref, 0)
+    weight_loads = [
+        load(wq_hbm, own.at[:, pl.ds(0, 32)], 1),
+        load(wf_hbm, own.at[:, pl.ds(32, 32)], 2),
+        load(wv_hbm, wv_ref, 3),
+        load(wg_hbm, wg_ref, 4),
+    ]
+    small_loads = [
+        load(wo_hbm.at[core], wo_ref, 5),
+        load(gain_hbm, gain_ref, 6),
+        load(floor_hbm, floor_ref, 7),
+        load(og_hbm, og_ref, 8),
+    ]
+    loads = [load(st_hbm.at[b], st.at[b], 9 + b) for b in range(2)]
+    x_load.wait()
     x_in = x_ref[...].astype(F32)
     x0[y, 8] = jnp.concatenate([x_in[8 * a : 8 * a + 8] for a in range(4)], axis=1).astype(BF16)
     pl.semaphore_wait(bar, len(zc) + len(yp) + len(dpp))
@@ -104,19 +121,21 @@
 
     for k, p in zip(zclose, zc):
         send(x0.at[y, 8], x0.at[y, 8 - k], sx.at[0, 0], rx.at[0, 0], p)
+    for copy in weight_loads:
+        copy.wait()
     for b in range(2):
-        own[b, 0:32, :] = wq_ref[b]
-        own[b, 32:64, :] = wf_ref[b]
         own[b, 64:96, :] = wv_ref[b].reshape(32, 256)
         own[b, 96:128, :] = wg_ref[b].reshape(32, 256)
         if b == 0:
             wt[dp] = own[0]
             for p in dpp:
                 send(own.at[0], wt.at[dp], sw.at[0], rw.at[0], p)
+    for copy in small_loads:
+        copy.wait()
     wide[turnover] = own[1, 0:64, :]
     wv1[x, core] = own[1, 64:128, :]
     for k in range(NZ):
-        wsrc[k] = wo_ref[core, :, :, 128 * k : 128 * k + 128].reshape(4, 8, 128)
+        wsrc[k] = wo_ref[:, :, 128 * k : 128 * k + 128].reshape(4, 8, 128)
     wo[core, z, y, x] = wsrc[z, x]
     spot = lax.broadcasted_iota(jnp.int32, (16, 128), 1) % 32
     head = lax.broadcasted_iota(jnp.int32, (16, 128), 0)
@@ -174,9 +193,12 @@
         if b == 0:
             proj = project(lambda d: wt[d], 128, inv)
             packed = turn([proj[8 * a : 8 * a + 8] for a in range(4)])
-            gq[y, z, 0] = packed[0].astype(BF16)
-            gq[y, z, 1] = packed[1].astype(BF16)
-            z_send(gq, 1)
+            gq[y, 8, 0] = packed[0].astype(BF16)
+            gq[y, 8, 1] = packed[1].astype(BF16)
+            for k in (8, 7, -7, 6, -6, 5, -5, 4, -4, 3, -3, 2, -2, 1, -1):
+                to = {"tp": lax.rem(z + NZ + k, NZ) * NY + y}
+                side = 0 if abs(k) > 4 else 2
+                send(gq.at[y, 8], gq.at[y, 8 - k], sx.at[1, side], rx.at[1, side], to)
             gate = packed[3]
         else:
             arrived(wq1.at[:, 0], sw.at[4], rw.at[4])
@@ -204,9 +226,14 @@
                 send(wo.at[core, :, y, x], wo.at[core, :, y, x], so_s.at[1], so_r.at[1], p)
         vt[...] = jnp.transpose(jnp.concatenate([proj, jnp.zeros((96, 128), F32)], axis=0))
         if b == 0:
-            z_wait(gq, 1)
-            y_send(gq, 1)
+            arrived(gq.at[0, pl.ds(0, 8)], sx.at[1, 2], rx.at[1, 2])
+            for p in yp:
+                send(gq.at[y, pl.ds(4, 9)], gq.at[y, pl.ds(4, 9)], sx.at[1, 1], rx.at[1, 1], p)
             z_send(gg.at[0], 2)
+            arrived(gq.at[0, pl.ds(0, 7)], sx.at[1, 0], rx.at[1, 0])
+            for p in yp:
+                send(gq.at[y, pl.ds(0, 4)], gq.at[y, pl.ds(0, 4)], sx.at[1, 1], rx.at[1, 1], p)
+                send(gq.at[y, pl.ds(13, 3)], gq.at[y, pl.ds(13, 3)], sx.at[1, 1], rx.at[1, 1], p)
             for k in (8, 4, 12):
                 to = {"tp": lax.rem(z + k, NZ) * NY + y}
                 send(own.at[1, pl.ds(0, 64)], wide.at[turnover], sw.at[1], rw.at[1], to)
@@ -220,7 +247,7 @@
             low = floor_ref[b : b + 1, 128 * k : 128 * k + 128]
             for p in range(2):
                 if b == 0:
-                    four = turn([gq[i, k, p].astype(F32) for i in range(NY)])
+                    four = turn([gq[i, lax.rem(k + 24 - z, NZ), p].astype(F32) for i in range(NY)])
                 else:
                     four = turn([gq1[(4 * i + k % 4) * 4 + k // 4, p].astype(F32) for i in range(NY)])
                 for a in range(4):
@@ -230,21 +257,34 @@
                     else:
                         kq[0, rows, :] = low + (1.0 - low) * (1.0 / (1.0 + jnp.exp(-four[a])))
         loads[b].wait()
+        if b == 0:
+            z_wait(gg.at[0], 2)
+            y_send(gg.at[0], 2)
         lane = lanes()
+        ones = jnp.ones((128, 128), BF16)
         read = [[jnp.zeros((8, 128), F32) for _ in range(2)] for _ in range(2)]
         first = 64 if b == 0 else 0
         vals = [[vt[pl.ds(first + 16 * hh + j, 8, stride=2), :] for hh in range(2)] for j in range(2)]
-        for s in range(32):
-            for hh in range(2):
-                keep = kq[0, s * PITCH + 8 * hh : s * PITCH + 8 * hh + 8, :]
-                quer = kq[1, s * PITCH + 8 * hh : s * PITCH + 8 * hh + 8, :]
-                rest = 1.0 - keep
-                for j in range(2):
-                    rows = pl.ds(s * 32 + hh * 16 + j, 8, stride=2)
-                    new = keep * st[b, rows, :] + rest * vals[j][hh][:, s : s + 1]
-                    st[b, rows, :] = new
-                    red = jnp.sum(quer * new, axis=1, keepdims=True)
-                    read[j][hh] = jnp.where(lane == s, red, read[j][hh])
+        for s0 in range(0, 32, 16):
+            terms = [[[], []], [[], []]]
+            for s in range(s0, s0 + 16):
+                for hh in range(2):
+                    keep = kq[0, s * PITCH + 8 * hh : s * PITCH + 8 * hh + 8, :]
+                    quer = kq[1, s * PITCH + 8 * hh : s * PITCH + 8 * hh + 8, :]
+                    rest = 1.0 - keep
+                    for j in range(2):
+                        rows = pl.ds(s * 32 + hh * 16 + j, 8, stride=2)
+                        new = keep * st[b, rows, :] + rest * vals[j][hh][:, s : s + 1]
+                        st[b, rows, :] = new
+                        terms[j][hh].append(quer * new)
+            for j in range(2):
+                for hh in range(2):
+                    term = jnp.concatenate(terms[j][hh], axis=0)
+                    high = term.astype(BF16)
+                    low = (term - high.astype(F32)).astype(BF16)
+                    sums = jnp.dot(high, ones, preferred_element_type=F32) + jnp.dot(low, ones, preferred_element_type=F32)
+                    for s in range(16):
+                        read[j][hh] = jnp.where(lane == s0 + s, sums[8 * s : 8 * s + 8], read[j][hh])
         vt[...] = jnp.zeros((128, 128), F32)
         for j in range(2):
             for hh in range(2):
@@ -256,8 +296,6 @@
         gr[b, y * NZ + z] = tile.astype(BF16)
         to_all(gr.at[b], base + 3)
         if b == 0:
-            z_wait(gg.at[0], 2)
-            y_send(gg.at[0], 2)
             arrived(wo.at[0, pl.ds(0, 12)], so_s.at[2], so_r.at[2])
             send(wo.at[core], wo.at[core], so_s.at[3], so_r.at[3], mate)
             arrived(wide.at[pl.ds(0, 3)], sw.at[1], rw.at[1])
@@ -305,7 +343,9 @@
     for b in range(2):
         all_left(gg.at[b], 4 * b + 2)
         left(gr.at[b, pl.ds(0, NY * NZ - 1)], sx.at[4 * b + 3, 0], rx.at[4 * b + 3, 0])
-    all_left(gq, 1)
+    left(gq.at[0, pl.ds(0, 7)], sx.at[1, 0], rx.at[1, 0])
+    left(gq.at[0, pl.ds(0, 8)], sx.at[1, 2], rx.at[1, 2])
+    left(gq.at[pl.ds(0, NY - 1)], sx.at[1, 1], rx.at[1, 1])
     left(gq1.at[pl.ds(0, 60)], sx.at[5, 0], rx.at[5, 0])
     left(x0.at[0, pl.ds(0, 8)], sx.at[0, 0], rx.at[0, 0])
     left(gr.at[0, pl.ds(0, 55)], sx.at[0, 1], rx.at[0, 1])
@@ -332,7 +372,7 @@
     new_resid, new_states = pl.pallas_call(
         kernel,
         out_shape=(pltpu.VMEM((32, 32), BF16), pltpu.VMEM(st.shape, F32)),
-        in_specs=[vmem] * 9 + [hbm],
+        in_specs=[hbm] * 10,
         out_specs=(vmem, vmem),
         scratch_shapes=[
             pltpu.VMEM((NY, NZ, 8, 128), BF16),
@@ -353,13 +393,20 @@
             pltpu.VMEM((NZ, 32, 128), F32),
             pltpu.VMEM((4, 8, 128), BF16),
             pltpu.VMEM((128, 128), F32),
-            dma((8, 2)),
-            dma((8, 2)),
+            pltpu.VMEM((32, 32), BF16),
+            pltpu.VMEM((2, 2048), F32),
+            pltpu.VMEM((2, 16, 2, 256), BF16),
+            pltpu.VMEM((2, 16, 2, 256), BF16),
+            pltpu.VMEM((2, 2048), F32),
+            pltpu.VMEM((2, 2, 16), F32),
+            pltpu.VMEM((16, 2, 2048), BF16),
+            dma((8, 3)),
+            dma((8, 3)),
             dma((6,)),
             dma((6,)),
             dma((4,)),
             dma((4,)),
-            dma((2,)),
+            dma((11,)),
         ],
         compiler_params=pltpu.CompilerParams(collective_id=0, has_side_effects=True),
         name="blocks",

time: 77.7 us -> 74.7 us (0.961)
  Pallas kernels: 75.3 us -> 71.9 us
    pallas_call x1, Pallas kernels: 75.3 us -> 71.9 us  [shards(): pl.pallas_call(kernel, out_shape=(pltpu.VMEM((32, 32), BF16), pltpu.VMEM(...]
where the time goes in v5:
time: 74.7 us; the launch traced here: 74.1 us
  Pallas kernels  71.9 us (96%)
  local copies, waits for them, and re-layouts  1.57 us (2%)
    pallas_call x1, Pallas kernels, shards(): pl.pallas_call(kernel, out_shape=(pltpu.VMEM((32, 32), BF16), pltpu.VMEM(...  71.9 us
    unnamed x2, local copies, waits for them, and re-layouts  1.57 us

profile of v5, /device:TPU:6, one launch (start us, length us, event | category | flops | bytes accessed | tf_op | source)
XLA Modules:
  0.0 74.1 jit_solution(12902786972927448910)
XLA Ops:
  0.6 71.9 %blocks.1 = (bf16[32,32]{1,0:T(8,128)(2,1)S(1)}, f32[2,1024,128]{2,1,0:T(8,128)S(1)}) custom-call(bf16[32,32]{1,0:T(8,128)(2,1)} %x_hbm.1, f32[2,2048]{1,0:T(2,128)} %gain_hbm.1, bf16[2,32,256]{2,1,0:T(8,128)(2,1)} %bitcast.9, bf16[2,32,256]{2,1,0:T(8,128)(2,1)} %bitcast.10, bf16[2,16,2,256]{3,2,1,0:T(2,128)(2,1)} %bitcast.11, ...), custom_call_target="tpu_custom_call" | custom-call | tf_op jit(solution)/shard_map/blocks/pallas_call | solution.py:372
  72.6 0.6 copy.14
  73.2 1.0 %copy.15 = f32[2,32,16,2,128]{4,3,2,1,0:T(2,128)} copy(f32[2,32,16,2,128]{4,3,2,1,0:T(2,128)S(1)} %bitcast.7) | data formatting | bytes 2097152

commit v6 on v5

--- a/solution.py
+++ b/solution.py
@@ -197,7 +197,7 @@
             gq[y, 8, 1] = packed[1].astype(BF16)
             for k in (8, 7, -7, 6, -6, 5, -5, 4, -4, 3, -3, 2, -2, 1, -1):
                 to = {"tp": lax.rem(z + NZ + k, NZ) * NY + y}
-                side = 0 if abs(k) > 4 else 2
+                side = 0 if abs(k) > 5 else 2
                 send(gq.at[y, 8], gq.at[y, 8 - k], sx.at[1, side], rx.at[1, side], to)
             gate = packed[3]
         else:
@@ -226,14 +226,14 @@
                 send(wo.at[core, :, y, x], wo.at[core, :, y, x], so_s.at[1], so_r.at[1], p)
         vt[...] = jnp.transpose(jnp.concatenate([proj, jnp.zeros((96, 128), F32)], axis=0))
         if b == 0:
-            arrived(gq.at[0, pl.ds(0, 8)], sx.at[1, 2], rx.at[1, 2])
+            arrived(gq.at[0, pl.ds(0, 10)], sx.at[1, 2], rx.at[1, 2])
             for p in yp:
-                send(gq.at[y, pl.ds(4, 9)], gq.at[y, pl.ds(4, 9)], sx.at[1, 1], rx.at[1, 1], p)
+                send(gq.at[y, pl.ds(3, 11)], gq.at[y, pl.ds(3, 11)], sx.at[1, 1], rx.at[1, 1], p)
             z_send(gg.at[0], 2)
-            arrived(gq.at[0, pl.ds(0, 7)], sx.at[1, 0], rx.at[1, 0])
+            arrived(gq.at[0, pl.ds(0, 5)], sx.at[1, 0], rx.at[1, 0])
             for p in yp:
-                send(gq.at[y, pl.ds(0, 4)], gq.at[y, pl.ds(0, 4)], sx.at[1, 1], rx.at[1, 1], p)
-                send(gq.at[y, pl.ds(13, 3)], gq.at[y, pl.ds(13, 3)], sx.at[1, 1], rx.at[1, 1], p)
+                send(gq.at[y, pl.ds(0, 3)], gq.at[y, pl.ds(0, 3)], sx.at[1, 1], rx.at[1, 1], p)
+                send(gq.at[y, pl.ds(14, 2)], gq.at[y, pl.ds(14, 2)], sx.at[1, 1], rx.at[1, 1], p)
             for k in (8, 4, 12):
                 to = {"tp": lax.rem(z + k, NZ) * NY + y}
                 send(own.at[1, pl.ds(0, 64)], wide.at[turnover], sw.at[1], rw.at[1], to)
@@ -343,8 +343,8 @@
     for b in range(2):
         all_left(gg.at[b], 4 * b + 2)
         left(gr.at[b, pl.ds(0, NY * NZ - 1)], sx.at[4 * b + 3, 0], rx.at[4 * b + 3, 0])
-    left(gq.at[0, pl.ds(0, 7)], sx.at[1, 0], rx.at[1, 0])
-    left(gq.at[0, pl.ds(0, 8)], sx.at[1, 2], rx.at[1, 2])
+    left(gq.at[0, pl.ds(0, 5)], sx.at[1, 0], rx.at[1, 0])
+    left(gq.at[0, pl.ds(0, 10)], sx.at[1, 2], rx.at[1, 2])
     left(gq.at[pl.ds(0, NY - 1)], sx.at[1, 1], rx.at[1, 1])
     left(gq1.at[pl.ds(0, 60)], sx.at[5, 0], rx.at[5, 0])
     left(x0.at[0, pl.ds(0, 8)], sx.at[0, 0], rx.at[0, 0])

time: 74.7 us -> 77.5 us (1.037)
  Pallas kernels: 71.9 us -> 75.1 us
    pallas_call x1, Pallas kernels: 71.9 us -> 75.1 us  [shards(): pl.pallas_call(kernel, out_shape=(pltpu.VMEM((32, 32), BF16), pltpu.VMEM(...]
where the time goes in v6:
time: 77.5 us; the launch traced here: 77.3 us
  Pallas kernels  75.1 us (97%)
  local copies, waits for them, and re-layouts  1.57 us (2%)
    pallas_call x1, Pallas kernels, shards(): pl.pallas_call(kernel, out_shape=(pltpu.VMEM((32, 32), BF16), pltpu.VMEM(...  75.1 us
    unnamed x2, local copies, waits for them, and re-layouts  1.57 us

profile of v6, /device:TPU:6, one launch (start us, length us, event | category | flops | bytes accessed | tf_op | source)
XLA Modules:
  0.0 77.3 jit_solution(8120792908494044137)
XLA Ops:
  0.6 75.1 %blocks.1 = (bf16[32,32]{1,0:T(8,128)(2,1)S(1)}, f32[2,1024,128]{2,1,0:T(8,128)S(1)}) custom-call(bf16[32,32]{1,0:T(8,128)(2,1)} %x_hbm.1, f32[2,2048]{1,0:T(2,128)} %gain_hbm.1, bf16[2,32,256]{2,1,0:T(8,128)(2,1)} %bitcast.9, bf16[2,32,256]{2,1,0:T(8,128)(2,1)} %bitcast.10, bf16[2,16,2,256]{3,2,1,0:T(2,128)(2,1)} %bitcast.11, ...), custom_call_target="tpu_custom_call" | custom-call | tf_op jit(solution)/shard_map/blocks/pallas_call | solution.py:372
  75.7 0.6 copy.14
  76.3 1.0 %copy.15 = f32[2,32,16,2,128]{4,3,2,1,0:T(2,128)} copy(f32[2,32,16,2,128]{4,3,2,1,0:T(2,128)S(1)} %bitcast.7) | data formatting | bytes 2097152
